TPU v7x, 32 devices: a whole 2x2x4 slice. The times are simulated.
32 devices in a mesh: st: 16 (over z, y, x), tp: 2 (over core).
Axes of the slice: x: 2, y: 2, z: 4, core: 2. Of those that a mesh axis runs over, the one named last changes fastest.
Arguments:
- hidden: bfloat16 [8192, 2048], P('st'), may hold values from -24 to 24
- passage_store: bfloat16 [512, 64, 2048], P('st'), may hold values from -6 to 6
- passage_ids: int32 [128, 4], P('st'), may hold values from 0 to 511, as said below
- query_weight: bfloat16 [2048, 512], P(None, 'tp'), may hold values from -0.125 to 0.125
- gate_weight: bfloat16 [2048, 512], P(None, 'tp'), may hold values from -0.125 to 0.125
- key_weight: bfloat16 [2048, 512], P(None, 'tp'), may hold values from -0.125 to 0.125
- value_weight: bfloat16 [2048, 512], P(None, 'tp'), may hold values from -0.125 to 0.125
- output_grad: bfloat16 [8192, 512], P('st', 'tp'), may hold values from -6 to 6
Outputs:
- grad_hidden: bfloat16 [8192, 2048], P(('st', 'tp'))
- grad_store: bfloat16 [512, 64, 2048], P(('st', 'tp'))
- grad_value_weight: float32 [2048, 512], P(None, 'tp')
Inputs may be any that keep to these rules, and one draw needn't show every extreme that they name: `passage_ids`: passage p is held at st index p // 32. The 32 ids of one index of st (its 8 blocks) are distinct; at most 4 of them name passages of one owner, and on every index some owner is named exactly 4 times. Every index reads at least one passage of the owner before it, of the owner after it and of the owner half the axis away.
All inputs are finite; a program needn't handle non-finite values.
Results may differ from a plain program's by a relative error of at most 0.012.
The roundings to bfloat16 on the way count: a program that leaves them out, or rounds other values in their place, can miss the bound.
Values may be sent and summed in bfloat16 or wider, within the bound.
A program may use at most 128 MiB of HBM per device.

v0:
```python
import functools

import jax
import jax.numpy as jnp
from jax import lax
from jax.experimental import pallas as pl
from jax.experimental.pallas import tpu as pltpu
from jax.sharding import PartitionSpec as P

HEAD_DIM = 256
NT = (((1,), (1,)), ((), ()))
TN = (((0,), (0,)), ((), ()))


def attend_kernel(per_block, span, heads, flat_ref, q_ref, gate_ref, up_ref, da_ref, k_ref, v_ref, dq_ref, dg_ref, dk_ref, dv_ref):
    b = pl.program_id(0)

    @pl.when(b == 0)
    def _():
        dk_ref[...] = jnp.zeros_like(dk_ref)
        dv_ref[...] = jnp.zeros_like(dv_ref)

    score_scale = HEAD_DIM ** (-0.5)
    slots = [flat_ref[b * per_block + j] for j in range(per_block)]
    keys = jnp.concatenate([k_ref[s] for s in slots], axis=0)
    values = jnp.concatenate([v_ref[s] for s in slots], axis=0)
    for h in range(heads):
        cols = slice(h * HEAD_DIM, (h + 1) * HEAD_DIM)
        k, v = keys[:, cols], values[:, cols]
        q, da = q_ref[:, cols], da_ref[:, cols]
        scores = lax.dot_general(q, k, NT, preferred_element_type=jnp.float32) * score_scale
        top = jnp.max(scores, axis=-1, keepdims=True)
        e = jnp.exp(scores - top)
        probs = e / jnp.sum(e, axis=-1, keepdims=True)
        probs_low = probs.astype(jnp.bfloat16)
        attended = jnp.dot(probs_low, v, preferred_element_type=jnp.float32)
        gates = gate_ref[:, cols]
        s = jax.nn.sigmoid(gates)
        up = up_ref[:, cols].astype(jnp.float32)
        dg_ref[:, cols] = (up * attended * s * (1.0 + gates * (1.0 - s))).astype(jnp.bfloat16)
        d_probs = lax.dot_general(da, v, NT, preferred_element_type=jnp.float32)
        centre = jnp.sum(probs * d_probs, axis=-1, keepdims=True)
        d_scores = (probs * (d_probs - centre) * score_scale).astype(jnp.bfloat16)
        dq_ref[:, cols] = jnp.dot(d_scores, k, preferred_element_type=jnp.float32).astype(
            jnp.bfloat16
        )
        d_keys = lax.dot_general(d_scores, q, TN, preferred_element_type=jnp.float32)
        d_values = lax.dot_general(probs_low, da, TN, preferred_element_type=jnp.float32)
        for j, slot in enumerate(slots):
            rows = slice(j * span, (j + 1) * span)
            dk_ref[slot, :, cols] = d_keys[rows].astype(jnp.bfloat16)
            dv_ref[slot, :, cols] = d_values[rows].astype(jnp.bfloat16)


def totals_kernel(unroll, held, passage_ref, came_ref, out_ref, acc):
    step = pl.program_id(0)

    @pl.when(step == 0)
    def _():
        acc[...] = jnp.zeros_like(acc)

    for u in range(unroll):
        acc[passage_ref[step * unroll + u]] += came_ref[u].astype(jnp.float32)

    @pl.when(step == pl.num_programs(0) - 1)
    def _():
        out_ref[...] = acc[:held].astype(jnp.bfloat16)


def body(
    hidden,
    passage_store,
    passage_ids,
    query_weight,
    gate_weight,
    key_weight,
    value_weight,
    output_grad,
):
    owner_count = lax.axis_size("st")
    tp_count = lax.axis_size("tp")
    tp_index = lax.axis_index("tp")
    held, span, model_width = passage_store.shape
    block_count, per_block = passage_ids.shape
    requests = block_count * per_block
    capacity = max(1, 2 * requests // owner_count)
    slot_total = owner_count * capacity
    width = query_weight.shape[1]
    heads = width // HEAD_DIM
    tokens = hidden.shape[0]
    block_rows = tokens // block_count
    bf16, f32 = jnp.bfloat16, jnp.float32
    exchange = [(i, tp_count - 1 - i) for i in range(tp_count)]

    ids = passage_ids.reshape(requests)
    owner_of = ids // held
    local_index = ids % held
    positions = jnp.arange(requests, dtype=jnp.int32)
    earlier = positions[None, :] < positions[:, None]
    rank = jnp.sum((owner_of[:, None] == owner_of[None, :]) & earlier, axis=1, dtype=jnp.int32)
    slot_flat = owner_of * capacity + rank
    code = local_index + 1
    hit = slot_flat[:, None] == jnp.arange(slot_total, dtype=jnp.int32)[None, :]
    table = jnp.sum(jnp.where(hit, code[:, None], 0), axis=0, dtype=jnp.int32)
    came = lax.all_to_all(
        table.reshape(owner_count, capacity), "st", split_axis=0, concat_axis=0, tiled=True
    ).reshape(slot_total)
    filled = came > 0
    slot_passage = jnp.maximum(came - 1, 0)
    slot_target = jnp.where(filled, slot_passage, held).astype(jnp.int32)

    store_rows = passage_store.reshape(held * span, model_width)

    def project(rows, weight):
        return jnp.dot(rows, weight, preferred_element_type=f32)

    keys_here = project(store_rows, key_weight).astype(bf16).reshape(held, span, width)
    values_here = project(store_rows, value_weight).astype(bf16).reshape(held, span, width)
    came_keys = lax.all_to_all(
        keys_here[slot_passage].reshape(owner_count, capacity, span, width),
        "st", split_axis=0, concat_axis=0, tiled=True,
    ).reshape(slot_total, span, width)
    came_values = lax.all_to_all(
        values_here[slot_passage].reshape(owner_count, capacity, span, width),
        "st", split_axis=0, concat_axis=0, tiled=True,
    ).reshape(slot_total, span, width)

    queries = project(hidden, query_weight).astype(bf16)
    gates = project(hidden, gate_weight)
    d_attended = (output_grad.astype(f32) * gates * jax.nn.sigmoid(gates)).astype(bf16)
    token_weight = jnp.concatenate([query_weight, gate_weight], axis=1)
    token_weight = jnp.concatenate(
        [token_weight, lax.ppermute(token_weight, "tp", exchange)], axis=1
    )
    row_weight = jnp.concatenate([key_weight, value_weight], axis=1)
    row_weight = jnp.concatenate([row_weight, lax.ppermute(row_weight, "tp", exchange)], axis=1)

    came_values, token_weight, row_weight = lax.optimization_barrier(
        (came_values, token_weight, row_weight)
    )

    whole3 = lambda b, f: (0, 0, 0)
    by_block = pl.BlockSpec((block_rows, width), lambda b, f: (b, 0))
    d_queries, d_gates, key_slots, value_slots = pl.pallas_call(
        functools.partial(attend_kernel, per_block, span, heads),
        grid_spec=pltpu.PrefetchScalarGridSpec(
            num_scalar_prefetch=1,
            grid=(block_count,),
            in_specs=[by_block] * 4 + [pl.BlockSpec((slot_total, span, width), whole3)] * 2,
            out_specs=[
                by_block,
                by_block,
                pl.BlockSpec((slot_total, span, width), whole3),
                pl.BlockSpec((slot_total, span, width), whole3),
            ],
        ),
        out_shape=[
            jax.ShapeDtypeStruct((tokens, width), bf16),
            jax.ShapeDtypeStruct((tokens, width), bf16),
            jax.ShapeDtypeStruct((slot_total, span, width), bf16),
            jax.ShapeDtypeStruct((slot_total, span, width), bf16),
        ],
        cost_estimate=pl.CostEstimate(flops=2_000_000_000, bytes_accessed=8_000_000, transcendentals=0),
        name="attend",
    )(slot_flat, queries, gates, output_grad, d_attended, came_keys, came_values)

    unroll = 8 if slot_total % 8 == 0 else 1

    def totals(slots):
        came = lax.all_to_all(
            slots.reshape(owner_count, capacity, span, width),
            "st", split_axis=0, concat_axis=0, tiled=True,
        ).reshape(slot_total, span, width)
        return pl.pallas_call(
            functools.partial(totals_kernel, unroll, held),
            grid_spec=pltpu.PrefetchScalarGridSpec(
                num_scalar_prefetch=1,
                grid=(slot_total // unroll,),
                in_specs=[pl.BlockSpec((unroll, span, width), lambda i, p: (i, 0, 0))],
                out_specs=pl.BlockSpec((held, span, width), lambda i, p: (0, 0, 0)),
                scratch_shapes=[pltpu.VMEM((held + 1, span, width), f32)],
            ),
            out_shape=jax.ShapeDtypeStruct((held, span, width), bf16),
            cost_estimate=pl.CostEstimate(
                flops=1_000_000_000, bytes_accessed=4_000_000, transcendentals=0
            ),
            name="totals",
        )(slot_target, came)

    value_low = totals(value_slots)
    key_low = totals(key_slots)

    def over_heads(first, second, weight):
        rows = jnp.concatenate([first, second], axis=1)
        half = rows.shape[0] // tp_count
        theirs = lax.dynamic_slice_in_dim(rows, (tp_count - 1 - tp_index) * half, half, 0)
        mine = lax.dynamic_slice_in_dim(rows, tp_index * half, half, 0)
        got = lax.ppermute(theirs, "tp", exchange)
        both = jnp.concatenate([mine, got], axis=1)
        return lax.dot_general(both, weight, NT, preferred_element_type=f32).astype(bf16)

    grad_hidden = over_heads(d_queries, d_gates, token_weight)

    value_rows = value_low.reshape(held * span, width)
    weight_part = lax.dot_general(store_rows, value_rows, TN, preferred_element_type=f32)
    parts = lax.all_to_all(
        weight_part.astype(bf16).reshape(owner_count, model_width // owner_count, width),
        "st", split_axis=0, concat_axis=0, tiled=True,
    )
    weight_sum = jnp.sum(parts.astype(f32), axis=0)
    shared = jnp.broadcast_to(weight_sum.astype(bf16)[None], parts.shape)
    grad_value_weight = (
        lax.all_to_all(shared, "st", split_axis=0, concat_axis=0, tiled=True)
        .reshape(model_width, width)
        .astype(f32)
    )

    grad_store = over_heads(key_low.reshape(held * span, width), value_rows, row_weight).reshape(
        held // tp_count, span, model_width
    )
    return (grad_hidden, grad_store, grad_value_weight)


def solution(mesh):
    placed = (
        P("st", None),
        P("st", None, None),
        P("st", None),
        P(None, "tp"),
        P(None, "tp"),
        P(None, "tp"),
        P(None, "tp"),
        P("st", "tp"),
    )
    return jax.shard_map(
        body,
        mesh=mesh,
        in_specs=placed,
        out_specs=(P(("st", "tp"), None), P(("st", "tp"), None, None), P(None, "tp")),
        check_vma=False,
    )
```

profile of v0, /device:TPU:8, one launch (start us, length us, event | category | flops | bytes accessed | tf_op | source)
XLA Modules:
  0.0 304.3 jit_solution(10790967857600902404)
XLA Ops:
  0.6 0.0 copy-start
  0.6 0.9 copy.18
  1.6 0.1 reshape.181
  1.6 0.2 convert_reduce_fusion
  1.8 0.0 copy-start.12
  1.8 0.1 select_reduce_fusion
  1.9 0.7 all_to_all.24
  2.6 7.2 %all-to-all-start = ((s32[16,1,4]{2,1,0:T(1,128)}), s32[16,1,4]{2,1,0:T(1,128)S(1)}, u32[]{:S(2)}, u32[]{:S(2)}) async-start(s32[16,1,4]{2,1,0:T(1,128)} %bitcast.2), calls=%async_computation | async-start | bytes 16384 | tf_op jit(solution)/shard_map/all_to_all | solution.py:105
  9.9 6.0 %convolution_convert_fusion.2 = bf16[2048,256]{1,0:T(8,128)(2,1)S(1)} fusion(bf16[2048,2048]{1,0:T(8,128)(2,1)} %bitcast.42, bf16[2048,256]{1,0:T(8,128)(2,1)} %param.14), kind=kOutput, calls=%fused_computation.8 | convolution fusion | flops 2148007936 | bytes 10485760 | tf_op jit(solution)/shard_map/dot_general | solution.py:115
  15.8 0.0 copy-done.12
  15.8 0.0 all-to-all-done
  15.8 0.1 fusion.11
  15.9 0.1 reshape.200
  16.0 2.0 gather_fusion.1
  18.0 6.9 %all-to-all-start.2 = ((bf16[16,4,64,256]{3,2,1,0:T(8,128)(2,1)}), bf16[16,4,64,256]{3,2,1,0:T(8,128)(2,1)}, u32[]{:S(2)}, u32[]{:S(2)}) async-start(bf16[16,4,64,256]{3,2,1,0:T(8,128)(2,1)} %bitcast.45), calls=%async_computation.2 | async-start | bytes 4194304 | tf_op jit(solution)/shard_map/all_to_all | solution.py:123
  24.9 6.0 %convolution_convert_fusion.3 = bf16[2048,256]{1,0:T(8,128)(2,1)S(1)} fusion(bf16[2048,2048]{1,0:T(8,128)(2,1)} %bitcast.43, bf16[2048,256]{1,0:T(8,128)(2,1)} %param.13), kind=kOutput, calls=%fused_computation.9 | convolution fusion | flops 2148007936 | bytes 10485760 | tf_op jit(solution)/shard_map/dot_general | solution.py:115
  30.9 2.0 gather_fusion
  32.9 39.1 %all-to-all-done.2 = bf16[16,4,64,256]{3,2,1,0:T(8,128)(2,1)} async-done(((bf16[16,4,64,256]{3,2,1,0:T(8,128)(2,1)}), bf16[16,4,64,256]{3,2,1,0:T(8,128)(2,1)}, u32[]{:S(2)}, u32[]{:S(2)}) %all-to-all-start.2) | async-done | bytes 2097184 | tf_op jit(solution)/shard_map/all_to_all | solution.py:123
  72.0 5.8 %all-to-all-start.1 = ((bf16[16,4,64,256]{3,2,1,0:T(8,128)(2,1)}), bf16[16,4,64,256]{3,2,1,0:T(8,128)(2,1)}, u32[]{:S(2)}, u32[]{:S(2)}) async-start(bf16[16,4,64,256]{3,2,1,0:T(8,128)(2,1)} %bitcast.44), calls=%async_computation.1 | async-start | bytes 4194304 | tf_op jit(solution)/shard_map/all_to_all | solution.py:119
  77.7 0.0 copy-done.4
  77.7 0.0 copy-start.6
  77.8 0.0 copy-start.7
  77.8 1.5 pad_maximum_fusion.3
  79.3 0.1 collective-permute-start.1
  79.4 0.0 copy-done.6
  79.4 0.2 copy-done.7
  79.6 0.2 pad_maximum_fusion.2
  79.8 0.0 copy-start.11
  79.8 0.3 collective-permute-start
  80.1 0.0 copy-done
  80.1 1.4 convolution_convert_fusion.4.q_ref
  81.5 0.0 copy-done.11
  81.5 1.6 multiply_convert_fusion
  83.2 0.4 collective-permute-done.1
  83.5 2.2 pad_maximum_fusion.1
  85.7 0.8 collective-permute-done
  86.5 2.3 pad_maximum_fusion
  88.8 35.8 %all-to-all-done.1 = bf16[16,4,64,256]{3,2,1,0:T(8,128)(2,1)} async-done(((bf16[16,4,64,256]{3,2,1,0:T(8,128)(2,1)}), bf16[16,4,64,256]{3,2,1,0:T(8,128)(2,1)}, u32[]{:S(2)}, u32[]{:S(2)}) %all-to-all-start.1) | async-done | bytes 2097184 | tf_op jit(solution)/shard_map/all_to_all | solution.py:119
  124.6 12.8 %attend.1 = (bf16[512,256]{1,0:T(8,128)(2,1)}, bf16[512,256]{1,0:T(8,128)(2,1)}, bf16[64,64,256]{2,1,0:T(8,128)(2,1)}, bf16[64,64,256]{2,1,0:T(8,128)(2,1)}) custom-call(s32[32]{0:T(128)} %copy-done.12, bf16[512,256]{1,0:T(8,128)(2,1)} %convolution_convert_fusion.4.q_ref, f32[512,256]{1,0:T(8,128)} %get-tuple-element.26.gate_ref, bf16[512,256]{1,0:T(8,128)(2,1)} %up_ref.1, ...), custom_call_target="tpu_custom_call" | custom-call | flops 2000000000 | bytes 8000000 | tf_op jit(solution)/shard_map/attend/pallas_call | solution.py:144
  137.4 53.3 %all_to_all.39 = bf16[16,4,64,256]{3,2,1,0:T(8,128)(2,1)} all-to-all(bf16[16,4,64,256]{3,2,1,0:T(8,128)(2,1)} %bitcast.49), channel_id=1, replica_groups=mesh['st'=16,'tp'=2] {'st'}, dimensions={0} | all-to-all | bytes 4194304 | tf_op jit(solution)/shard_map/all_to_all | solution.py:170
  190.7 5.0 %all-to-all-start.3 = ((bf16[16,4,64,256]{3,2,1,0:T(8,128)(2,1)}), bf16[16,4,64,256]{3,2,1,0:T(8,128)(2,1)}, u32[]{:S(2)}, u32[]{:S(2)}) async-start(bf16[16,4,64,256]{3,2,1,0:T(8,128)(2,1)} %bitcast.8), calls=%async_computation.3 | async-start | bytes 4194304 | tf_op jit(solution)/shard_map/all_to_all | solution.py:170
  195.6 0.6 select_n.57.passage_ref
  196.2 6.2 %totals.3 = bf16[32,64,256]{2,1,0:T(8,128)(2,1)} custom-call(s32[64]{0:T(128)} %select_n.57.passage_ref, bf16[64,64,256]{2,1,0:T(8,128)(2,1)} %bitcast.50), custom_call_target="tpu_custom_call" | custom-call | flops 1000000000 | bytes 4000000 | tf_op jit(solution)/shard_map/totals/pallas_call | solution.py:174
  202.4 6.1 %fusion.4 = bf16[32,16,8,128]{3,2,1,0:T(8,128)(2,1)S(1)} fusion(bf16[32,64,256]{2,1,0:T(8,128)(2,1)} %totals.3, bf16[32,64,2048]{2,1,0:T(8,128)(2,1)} %param.9), kind=kOutput, calls=%fused_computation.19 | convolution fusion | flops 2148007936 | bytes 10485760 | tf_op jit(solution)/shard_map/dot_general | solution.py:205
  208.5 1.2 copy.26
  209.8 32.3 %all-to-all-done.3 = bf16[16,4,64,256]{3,2,1,0:T(8,128)(2,1)} async-done(((bf16[16,4,64,256]{3,2,1,0:T(8,128)(2,1)}), bf16[16,4,64,256]{3,2,1,0:T(8,128)(2,1)}, u32[]{:S(2)}, u32[]{:S(2)}) %all-to-all-start.3) | async-done | bytes 2097184 | tf_op jit(solution)/shard_map/all_to_all | solution.py:170
  242.1 5.6 %all-to-all-start.5 = ((bf16[16,128,256]{1,2,0:T(8,128)(2,1)}), bf16[16,128,256]{1,2,0:T(8,128)(2,1)S(1)}, u32[]{:S(2)}, u32[]{:S(2)}) async-start(bf16[16,128,256]{1,2,0:T(8,128)(2,1)} %bitcast.41), calls=%async_computation.5 | async-start | bytes 2097152 | tf_op jit(solution)/shard_map/all_to_all | solution.py:206
  247.7 6.2 %totals.2 = bf16[32,64,256]{2,1,0:T(8,128)(2,1)} custom-call(s32[64]{0:T(128)} %select_n.57.passage_ref, bf16[64,64,256]{2,1,0:T(8,128)(2,1)} %bitcast.9.came_ref), custom_call_target="tpu_custom_call" | custom-call | flops 1000000000 | bytes 4000000 | tf_op jit(solution)/shard_map/totals/pallas_call | solution.py:174
  254.0 2.7 fusion.6
  256.7 0.0 collective-permute-start.3
  256.7 15.9 %all-to-all-done.5 = bf16[16,128,256]{1,2,0:T(8,128)(2,1)S(1)} async-done(((bf16[16,128,256]{1,2,0:T(8,128)(2,1)}), bf16[16,128,256]{1,2,0:T(8,128)(2,1)S(1)}, u32[]{:S(2)}, u32[]{:S(2)}) %all-to-all-start.5) | async-done | bytes 1048608 | tf_op jit(solution)/shard_map/all_to_all | solution.py:206
  272.5 0.1 reduce_sum.32
  272.7 0.1 copy.22
  272.8 1.1 broadcast_in_dim.18
  273.9 4.7 %all-to-all-start.6 = ((bf16[16,128,256]{2,1,0:T(8,128)(2,1)}), bf16[16,128,256]{2,1,0:T(8,128)(2,1)S(1)}, u32[]{:S(2)}, u32[]{:S(2)}) async-start(bf16[16,128,256]{2,1,0:T(8,128)(2,1)} %broadcast_in_dim.18), calls=%async_computation.6 | async-start | bytes 2097152 | tf_op jit(solution)/shard_map/all_to_all | solution.py:213
  278.6 0.0 copy-done.9
  278.7 0.1 collective-permute-start.2
  278.8 1.5 collective-permute-done.2
  280.3 4.6 %convolution_convert_fusion.1 = bf16[256,2048]{1,0:T(8,128)(2,1)} fusion(bf16[2048,1024]{1,0:T(8,128)(2,1)} %pad_maximum_fusion, bf16[256,512]{1,0:T(8,128)(2,1)S(1)} %collective-permute-done.2, bf16[256,512]{1,0:T(8,128)(2,1)S(1)} %get-tuple-element.21), kind=kOutput, calls=%fused_computation.6 | convolution fusion | flops 1075314688 | bytes 5767168 | tf_op jit(solution)/shard_map/dot_general | solution.py:200
  284.9 0.0 collective-permute-done.3
  285.0 0.0 copy-start.1
  285.0 7.5 %convolution_convert_fusion = bf16[1024,2048]{1,0:T(8,128)(2,1)} fusion(bf16[2048,1024]{1,0:T(8,128)(2,1)S(1)} %copy-done.3, bf16[1024,512]{1,0:T(8,128)(2,1)} %collective-permute-done.3, bf16[1024,512]{1,0:T(8,128)(2,1)S(1)} %copy-done.8), kind=kOutput, calls=%fused_computation.4 | convolution fusion | flops 4301258752 | bytes 10485760 | tf_op jit(solution)/shard_map/dot_general | solution.py:200
  292.4 10.3 %all-to-all-done.6 = bf16[16,128,256]{2,1,0:T(8,128)(2,1)S(1)} async-done(((bf16[16,128,256]{2,1,0:T(8,128)(2,1)}), bf16[16,128,256]{2,1,0:T(8,128)(2,1)S(1)}, u32[]{:S(2)}, u32[]{:S(2)}) %all-to-all-start.6) | async-done | bytes 1048608 | tf_op jit(solution)/shard_map/all_to_all | solution.py:213
  302.7 1.5 bitcast_convert_fusion
  (19 shorter events, 0.1 us)
Async XLA Ops:
  0.6 79.5 %copy-start = (bf16[512,2048]{1,0:T(8,128)(2,1)S(1)}, bf16[512,2048]{1,0:T(8,128)(2,1)}, u32[]{:S(2)}) copy-start(bf16[512,2048]{1,0:T(8,128)(2,1)} %param.8) | copy-start | bytes 6291460
  1.8 14.0 %copy-start.12 = (s32[32]{0:T(128)}, s32[32]{0:T(128)S(1)}, u32[]{:S(2)}) copy-start(s32[32]{0:T(128)S(1)} %multiply_add_fusion.flat_ref) | copy-start | bytes 388
  2.6 13.2 %all-to-all-start = ((s32[16,1,4]{2,1,0:T(1,128)}), s32[16,1,4]{2,1,0:T(1,128)S(1)}, u32[]{:S(2)}, u32[]{:S(2)}) async-start(s32[16,1,4]{2,1,0:T(1,128)} %bitcast.2), calls=%async_computation | async-start | bytes 16384 | tf_op jit(solution)/shard_map/all_to_all | solution.py:105
  18.0 53.9 %all-to-all-start.2 = ((bf16[16,4,64,256]{3,2,1,0:T(8,128)(2,1)}), bf16[16,4,64,256]{3,2,1,0:T(8,128)(2,1)}, u32[]{:S(2)}, u32[]{:S(2)}) async-start(bf16[16,4,64,256]{3,2,1,0:T(8,128)(2,1)} %bitcast.45), calls=%async_computation.2 | async-start | bytes 4194304 | tf_op jit(solution)/shard_map/all_to_all | solution.py:123
  72.0 5.8 %copy-start.4 = (bf16[2048,256]{1,0:T(8,128)(2,1)S(1)}, bf16[2048,256]{1,0:T(8,128)(2,1)}, u32[]{:S(2)}) copy-start(bf16[2048,256]{1,0:T(8,128)(2,1)} %param.13) | copy-start | bytes 3145732
  72.0 52.6 %all-to-all-start.1 = ((bf16[16,4,64,256]{3,2,1,0:T(8,128)(2,1)}), bf16[16,4,64,256]{3,2,1,0:T(8,128)(2,1)}, u32[]{:S(2)}, u32[]{:S(2)}) async-start(bf16[16,4,64,256]{3,2,1,0:T(8,128)(2,1)} %bitcast.44), calls=%async_computation.1 | async-start | bytes 4194304 | tf_op jit(solution)/shard_map/all_to_all | solution.py:119
  77.7 1.6 copy-start.6
  77.8 1.8 copy-start.7
  79.3 4.2 %collective-permute-start.1 = (bf16[2048,512]{1,0:T(8,128)(2,1)S(1)}, bf16[2048,512]{1,0:T(8,128)(2,1)S(1)}, u32[]{:S(2)}, u32[]{:S(2)}) collective-permute-start(bf16[2048,512]{1,0:T(8,128)(2,1)S(1)} %pad_maximum_fusion.3), channel_id=1, source_target_pairs={{0,1},{1,0},{2,3},{3,2},{4,5},{5,4},{6,7},{7,6},{8,9},{9,8},{10,11... | collective-permute-start | bytes 6291464 | tf_op jit(solution)/shard_map/ppermute | solution.py:136
  79.8 1.8 copy-start.11
  79.8 6.7 %collective-permute-start = (bf16[2048,512]{1,0:T(8,128)(2,1)S(1)}, bf16[2048,512]{1,0:T(8,128)(2,1)S(1)}, u32[]{:S(2)}, u32[]{:S(2)}) collective-permute-start(bf16[2048,512]{1,0:T(8,128)(2,1)S(1)} %pad_maximum_fusion.2), channel_id=1, source_target_pairs={{0,1},{1,0},{2,3},{3,2},{4,5},{5,4},{6,7},{7,6},{8,9},{9,8},{10,11... | collective-permute-start | bytes 6291464 | tf_op jit(solution)/shard_map/ppermute | solution.py:133
  81.5 2.0 copy-start.5
  190.7 51.4 %all-to-all-start.3 = ((bf16[16,4,64,256]{3,2,1,0:T(8,128)(2,1)}), bf16[16,4,64,256]{3,2,1,0:T(8,128)(2,1)}, u32[]{:S(2)}, u32[]{:S(2)}) async-start(bf16[16,4,64,256]{3,2,1,0:T(8,128)(2,1)} %bitcast.8), calls=%async_computation.3 | async-start | bytes 4194304 | tf_op jit(solution)/shard_map/all_to_all | solution.py:170
  242.1 30.4 %all-to-all-start.5 = ((bf16[16,128,256]{1,2,0:T(8,128)(2,1)}), bf16[16,128,256]{1,2,0:T(8,128)(2,1)S(1)}, u32[]{:S(2)}, u32[]{:S(2)}) async-start(bf16[16,128,256]{1,2,0:T(8,128)(2,1)} %bitcast.41), calls=%async_computation.5 | async-start | bytes 2097152 | tf_op jit(solution)/shard_map/all_to_all | solution.py:206
  247.7 6.2 %copy-start.2 = (bf16[32,64,256]{2,1,0:T(8,128)(2,1)S(1)}, bf16[32,64,256]{2,1,0:T(8,128)(2,1)}, u32[]{:S(2)}) copy-start(bf16[32,64,256]{2,1,0:T(8,128)(2,1)} %totals.3) | copy-start | bytes 3145732
  256.7 21.9 %copy-start.10 = (bf16[512,256]{1,0:T(8,128)(2,1)S(1)}, bf16[512,256]{1,0:T(8,128)(2,1)}, u32[]{:S(2)}) copy-start(bf16[512,256]{1,0:T(8,128)(2,1)} %get-tuple-element.11) | copy-start | bytes 786436
  256.7 28.3 %collective-permute-start.3 = (bf16[1024,512]{1,0:T(8,128)(2,1)}, bf16[1024,512]{1,0:T(8,128)(2,1)}, u32[]{:S(2)}, u32[]{:S(2)}) collective-permute-start(bf16[1024,512]{1,0:T(8,128)(2,1)} %get-tuple-element.20), channel_id=1, source_target_pairs={{0,1},{1,0},{2,3},{3,2},{4,5},{5,4},{6,7},{7,6},{8,9},{9,8},{10,11... | collective-permute-start | bytes 3145736 | tf_op jit(solution)/shard_map/ppermute | solution.py:198
  272.7 6.0 %copy-start.9 = (bf16[512,256]{1,0:T(8,128)(2,1)S(1)}, bf16[512,256]{1,0:T(8,128)(2,1)}, u32[]{:S(2)}) copy-start(bf16[512,256]{1,0:T(8,128)(2,1)} %get-tuple-element.12) | copy-start | bytes 786436
  273.9 28.8 %all-to-all-start.6 = ((bf16[16,128,256]{2,1,0:T(8,128)(2,1)}), bf16[16,128,256]{2,1,0:T(8,128)(2,1)S(1)}, u32[]{:S(2)}, u32[]{:S(2)}) async-start(bf16[16,128,256]{2,1,0:T(8,128)(2,1)} %broadcast_in_dim.18), calls=%async_computation.6 | async-start | bytes 2097152 | tf_op jit(solution)/shard_map/all_to_all | solution.py:213
  278.7 1.6 collective-permute-start.2
  280.3 4.6 %copy-start.3 = (bf16[2048,1024]{1,0:T(8,128)(2,1)S(1)}, bf16[2048,1024]{1,0:T(8,128)(2,1)}, u32[]{:S(2)}) copy-start(bf16[2048,1024]{1,0:T(8,128)(2,1)} %pad_maximum_fusion.1) | copy-start | bytes 12582916
  280.3 4.6 %copy-start.8 = (bf16[1024,512]{1,0:T(8,128)(2,1)S(1)}, bf16[1024,512]{1,0:T(8,128)(2,1)}, u32[]{:S(2)}) copy-start(bf16[1024,512]{1,0:T(8,128)(2,1)} %get-tuple-element.19) | copy-start | bytes 3145732
  285.0 19.3 %copy-start.1 = (bf16[512,2048]{1,0:T(8,128)(2,1)S(1)}, bf16[512,2048]{1,0:T(8,128)(2,1)}, u32[]{:S(2)}) copy-start(bf16[512,2048]{1,0:T(8,128)(2,1)} %param.8) | copy-start | bytes 6291460
where the time goes:
time: 305 us; the launch traced here: 304 us
  waiting for transfers between devices  136 us (45%)
  blocking collectives  53.3 us (17%)
  starting transfers between devices  35.7 us (12%)
  matrix products  33.1 us (11%)
  Pallas kernels  25.2 us (8%)
  other arithmetic  11 us (4%)
  local copies, waits for them, and re-layouts  9.17 us (3%)
    all_to_all x1, blocking collectives, totals(): lax.all_to_all(slots.reshape(owner_count, capacity, span, width), 'st', s...  53.3 us
    all_to_all x1, waiting for transfers between devices, body(): lax.all_to_all(values_here[slot_passage].reshape(owner_count, capacity, s...  39.1 us
    all_to_all x1, waiting for transfers between devices, body(): lax.all_to_all(keys_here[slot_passage].reshape(owner_count, capacity, spa...  35.8 us
    all_to_all x1, waiting for transfers between devices, totals(): lax.all_to_all(slots.reshape(owner_count, capacity, span, width), 'st', s...  32.3 us
    all_to_all x1, waiting for transfers between devices, body(): lax.all_to_all(weight_part.astype(bf16).reshape(owner_count, model_width...  15.9 us
    dot_general x4, matrix products, project(): return jnp.dot(rows, weight, preferred_element_type=f32)  14.9 us
    pallas_call x1, Pallas kernels, body(): pl.pallas_call(functools.partial(attend_kernel, per_block, span, heads),...  12.8 us
    pallas_call x2, Pallas kernels, totals(): pl.pallas_call(functools.partial(totals_kernel, unroll, held), grid_spec=...  12.4 us
  transfers between devices with their start and end apart: 10, of which 8 were waited for; matrix products, arithmetic and copies ran while one was open for 16% of the time, Pallas kernels for 4%

commit v1 on v0

v1 whole, which is shorter than its diff:
```python
import functools
import math

import jax
import jax.numpy as jnp
from jax import lax
from jax.experimental import pallas as pl
from jax.experimental.pallas import tpu as pltpu
from jax.sharding import PartitionSpec as P

HEAD_DIM = 256
NT = (((1,), (1,)), ((), ()))
TN = (((0,), (0,)), ((), ()))
MESH = pl.DeviceIdType.MESH
UNROLL = 4
CHUNKS = 8
LOW = -1e30
bf16, f32, i32 = jnp.bfloat16, jnp.float32, jnp.int32
ANY = pl.BlockSpec(memory_space=pl.ANY)
VM = pl.BlockSpec(memory_space=pltpu.VMEM)


def greet(peers):
    barrier = pltpu.get_barrier_semaphore()
    for peer in peers:
        pl.semaphore_signal(barrier, inc=1, device_id={"st": peer}, device_id_type=MESH)
    pl.semaphore_wait(barrier, len(peers))


def place(depth, plane):
    me = lax.axis_index("st")
    my_z, my_p = me // plane, me % plane
    column = [((my_z + d) % depth) * plane + my_p for d in range(1, depth)]
    row = [my_z * plane + (my_p + d) % plane for d in range(1, plane)]
    return me, my_z, my_p, column, row


def remote(src, dst, send, recv, peer):
    return pltpu.make_async_remote_copy(
        src_ref=src, dst_ref=dst, send_sem=send, recv_sem=recv,
        device_id={"st": peer}, device_id_type=MESH,
    )


def forward_kernel(
    depth, plane, cap, held,
    table, hidden_hbm, store_hbm, wq_hbm, wg_hbm, wk_hbm, wv_hbm, up_hbm,
    qa_all, kv_all, gate_ref,
    hidden, store, wq, wg, wk, wv, up, qa, keys, values, pack,
    load_sem, chunk_sem, own_sem, zsend, zrecv, psend, precv,
):
    me, my_z, my_p, column, row = place(depth, plane)
    owners = depth * plane
    rows = store.shape[0] // CHUNKS
    span, width = keys.shape[1:]
    passages = rows // span
    loads = [
        pltpu.make_async_copy(a, b, load_sem.at[i])
        for i, (a, b) in enumerate(
            ((hidden_hbm, hidden), (wq_hbm, wq), (wg_hbm, wg), (up_hbm, up), (wk_hbm, wk), (wv_hbm, wv))
        )
    ]
    for c in loads:
        c.start()

    def chunk(c):
        at = pl.ds(pl.multiple_of(c * rows, rows), rows)
        return pltpu.make_async_copy(store_hbm.at[at], store.at[at], chunk_sem.at[c])

    for c in range(CHUNKS):
        chunk(c).start()
    greet(column + row)

    loads[0].wait()
    loads[1].wait()
    qa[0] = jnp.dot(hidden[...], wq[...], preferred_element_type=f32).astype(bf16)
    loads[2].wait()
    loads[3].wait()
    gates = jnp.dot(hidden[...], wg[...], preferred_element_type=f32)
    gate_ref[...] = gates
    qa[1] = (up[...].astype(f32) * gates * jax.nn.sigmoid(gates)).astype(bf16)
    z_copies = [
        remote(qa, qa_all.at[my_z], zsend.at[i], zrecv.at[i], peer) for i, peer in enumerate(column)
    ]
    for c in z_copies:
        c.start()
    own_q = pltpu.make_async_copy(qa, qa_all.at[my_z], own_sem.at[0])
    own_q.start()

    loads[4].wait()
    loads[5].wait()

    @pl.loop(0, CHUNKS)
    def _(c):
        chunk(c).wait()
        part = store[pl.ds(pl.multiple_of(c * rows, rows), rows)]
        at = pl.ds(c * passages, passages)
        keys[at] = jnp.dot(part, wk[...], preferred_element_type=f32).astype(bf16).reshape(
            passages, span, width
        )
        values[at] = jnp.dot(part, wv[...], preferred_element_type=f32).astype(bf16).reshape(
            passages, span, width
        )

    slots = depth * cap
    p_copies = []
    for i in range(plane):
        peer = me if i == plane - 1 else row[i]
        peer_p = peer % plane

        @pl.loop(0, slots)
        def _(s):
            reader = (s // cap) * plane + peer_p
            code = table[(reader * owners + me) * cap + s % cap]
            local = jnp.maximum(code - 1, 0) % held
            pack[i, 0, s] = keys[local]
            pack[i, 1, s] = values[local]

        if i == plane - 1:
            own_kv = pltpu.make_async_copy(pack.at[i], kv_all.at[my_p], own_sem.at[1])
            own_kv.start()
        else:
            c = remote(pack.at[i], kv_all.at[my_p], psend.at[i], precv.at[i], peer)
            c.start()
            p_copies.append(c)
    own_q.wait()
    own_kv.wait()
    for c in z_copies + p_copies:
        c.wait()


def listed(sizes, table, me, slot_list, pos_list, acc_list):
    depth, plane, cap, held, requests, per_block = sizes
    owners, slots = depth * plane, depth * cap
    blocks = depth * requests // per_block

    def step(s, n):
        p, zc = s // slots, s % slots
        reader = (zc // cap) * plane + me % plane
        owner = (me // plane) * plane + p
        code = table[(reader * owners + owner) * cap + zc % cap]
        pos = (zc // cap) * requests + jnp.maximum(code - 1, 0) // held
        slot_list[n] = s
        pos_list[n] = pos
        acc_list[n] = pos // per_block
        return n + (code > 0).astype(i32)

    n = lax.fori_loop(0, plane * slots, step, jnp.int32(0))
    last = jnp.maximum(n - 1, 0)
    for u in range(UNROLL):
        slot_list[n + u] = slot_list[last]
        pos_list[n + u] = pos_list[last]
        acc_list[n + u] = blocks
    return (n + UNROLL - 1) // UNROLL


def operands(sizes, kv_ref, qa_ref, slot, block):
    depth, _, cap, _, requests, per_block = sizes
    slots, per_reader = depth * cap, requests // per_block
    p, zc = slot // slots, slot % slots
    z, b = block // per_reader, block % per_reader
    return kv_ref[p, 0, zc], kv_ref[p, 1, zc], qa_ref[z, 0, b], qa_ref[z, 1, b]


def stats_kernel(sizes, table, kv_ref, qa_ref, out_ref, tops, sums, mids, slot_list, pos_list, acc_list):
    per_block = sizes[-1]
    blocks = sizes[0] * sizes[4] // per_block
    span = qa_ref.shape[3]
    scale = HEAD_DIM ** (-0.5)
    tops[...] = jnp.full_like(tops, LOW)
    sums[...] = jnp.zeros_like(sums)
    mids[...] = jnp.zeros_like(mids)
    trips = listed(sizes, table, lax.axis_index("st"), slot_list, pos_list, acc_list)

    @pl.loop(0, trips)
    def _(t):
        found = []
        for u in range(UNROLL):
            pos = pos_list[t * UNROLL + u]
            block = pos // per_block
            k, v, q, da = operands(sizes, kv_ref, qa_ref, slot_list[t * UNROLL + u], block)
            scores = lax.dot_general(k, q, NT, preferred_element_type=f32) * scale
            d_probs = lax.dot_general(v, da, NT, preferred_element_type=f32)
            top = jnp.max(scores, axis=0, keepdims=True)
            e = jnp.exp(scores - top)
            found.append((
                pos % per_block, block, top,
                jnp.sum(e, axis=0, keepdims=True), jnp.sum(e * d_probs, axis=0, keepdims=True),
            ))
        for j, block, top, total, mid in found:
            tops[j, pl.ds(block, 1), :] = top
            sums[j, pl.ds(block, 1), :] = total
            mids[j, pl.ds(block, 1), :] = mid

    top = jnp.max(tops[...], axis=0)
    ratio = jnp.exp(tops[...] - top[None])
    out_ref[0:blocks, 0:span] = top
    out_ref[0:blocks, span:] = jnp.sum(sums[...] * ratio, axis=0)
    out_ref[blocks:, 0:span] = jnp.sum(mids[...] * ratio, axis=0)
    out_ref[blocks:, span:] = jnp.zeros_like(top)


def share_kernel(depth, plane, own_ref, all_ref, send, recv):
    _, my_z, _, column, _ = place(depth, plane)
    greet(column)
    copies = [remote(own_ref, all_ref.at[my_z], send.at[i], recv.at[i], p) for i, p in enumerate(column)]
    for c in copies:
        c.start()
    all_ref[my_z] = own_ref[...]
    for c in copies:
        c.wait()


def grads_kernel(sizes, table, kv_ref, qa_ref, stats_ref, dkv_ref, part_ref, acc, top_at, inv_at, mid_at, slot_list, pos_list, acc_list):
    depth, _, cap, _, requests, per_block = sizes
    slots, per_reader = depth * cap, requests // per_block
    blocks = depth * per_reader
    span = qa_ref.shape[3]
    scale = HEAD_DIM ** (-0.5)
    trips = listed(sizes, table, lax.axis_index("st"), slot_list, pos_list, acc_list)
    acc[...] = jnp.zeros_like(acc)
    tops = [stats_ref[z, 0:blocks, 0:span] for z in range(depth)]
    top = functools.reduce(jnp.maximum, tops)
    ratios = [jnp.exp(t - top) for t in tops]
    total = sum(stats_ref[z, 0:blocks, span:] * ratios[z] for z in range(depth))
    mid = sum(stats_ref[z, blocks:, 0:span] * ratios[z] for z in range(depth))
    inverse = 1.0 / total
    top_at[...] = top
    inv_at[...] = inverse
    mid_at[...] = mid * inverse

    @pl.loop(0, trips)
    def _(t):
        for u in range(UNROLL):
            slot = slot_list[t * UNROLL + u]
            block = pos_list[t * UNROLL + u] // per_block
            k, v, q, da = operands(sizes, kv_ref, qa_ref, slot, block)
            scores = lax.dot_general(k, q, NT, preferred_element_type=f32) * scale
            d_probs = lax.dot_general(v, da, NT, preferred_element_type=f32)
            probs = jnp.exp(scores - top_at[pl.ds(block, 1), :]) * inv_at[pl.ds(block, 1), :]
            low = probs.astype(bf16)
            d_scores = (probs * (d_probs - mid_at[pl.ds(block, 1), :]) * scale).astype(bf16)
            p, zc = slot // slots, slot % slots
            dkv_ref[p, 0, zc] = jnp.dot(d_scores, q, preferred_element_type=f32).astype(bf16)
            dkv_ref[p, 1, zc] = jnp.dot(low, da, preferred_element_type=f32).astype(bf16)
            at = acc_list[t * UNROLL + u]
            acc[0, at] += lax.dot_general(low, v, TN, preferred_element_type=f32)
            acc[1, at] += lax.dot_general(d_scores, k, TN, preferred_element_type=f32)

    for z in range(depth):
        part_ref[z, 0] = acc[0, z * per_reader : (z + 1) * per_reader].astype(bf16)
        part_ref[z, 1] = acc[1, z * per_reader : (z + 1) * per_reader].astype(bf16)


def back_kernel(depth, plane, dkv, part, dkv_in, part_in, kv_buf, part_buf, own_sem, zsend, zrecv, psend, precv):
    me, my_z, my_p, column, row = place(depth, plane)
    first = [
        pltpu.make_async_copy(dkv.at[my_p], kv_buf, own_sem.at[0]),
        pltpu.make_async_copy(part.at[my_z], part_buf, own_sem.at[1]),
    ]
    for c in first:
        c.start()
    greet(column + row)
    copies = [
        remote(dkv.at[peer % plane], dkv_in.at[my_p], psend.at[i], precv.at[i], peer)
        for i, peer in enumerate(row)
    ] + [
        remote(part.at[peer // plane], part_in.at[my_z], zsend.at[i], zrecv.at[i], peer)
        for i, peer in enumerate(column)
    ]
    for c in copies:
        c.start()
    for c in first:
        c.wait()
    second = [
        pltpu.make_async_copy(kv_buf, dkv_in.at[my_p], own_sem.at[2]),
        pltpu.make_async_copy(part_buf, part_in.at[my_z], own_sem.at[3]),
    ]
    for c in second:
        c.start()
    for c in second + copies:
        c.wait()


def totals_kernel(sizes, table, dkv_ref, key_ref, value_ref, acc):
    depth, plane, cap, held, _, _ = sizes
    owners, slots = depth * plane, depth * cap
    me = lax.axis_index("st")
    acc[...] = jnp.zeros_like(acc)

    @pl.loop(0, plane * slots)
    def _(s):
        p, zc = s // slots, s % slots
        code = table[(((zc // cap) * plane + p) * owners + me) * cap + zc % cap]

        @pl.when(code > 0)
        def _():
            at = (code - 1) % held
            acc[0, at] += dkv_ref[p, 0, zc].astype(f32)
            acc[1, at] += dkv_ref[p, 1, zc].astype(f32)

    key_ref[...] = acc[0].astype(bf16)
    value_ref[...] = acc[1].astype(bf16)


def body(
    hidden,
    passage_store,
    passage_ids,
    query_weight,
    gate_weight,
    key_weight,
    value_weight,
    output_grad,
):
    owner_count = lax.axis_size("st")
    tp_count = lax.axis_size("tp")
    tp_index = lax.axis_index("tp")
    depth = 2 ** ((int(math.log2(owner_count)) + 1) // 2)
    plane = owner_count // depth
    held, span, model_width = passage_store.shape
    block_count, per_block = passage_ids.shape
    requests = block_count * per_block
    cap = max(1, 2 * requests // owner_count)
    width = query_weight.shape[1]
    tokens = hidden.shape[0]
    block_rows = tokens // block_count
    slots = depth * cap
    blocks = depth * block_count
    sizes = (depth, plane, cap, held, requests, per_block)
    exchange = [(i, tp_count - 1 - i) for i in range(tp_count)]
    sds = jax.ShapeDtypeStruct

    ids = passage_ids.reshape(requests)
    owner_of = ids // held
    positions = jnp.arange(requests, dtype=i32)
    earlier = positions[None, :] < positions[:, None]
    rank = jnp.sum((owner_of[:, None] == owner_of[None, :]) & earlier, axis=1, dtype=i32)
    code = positions * held + ids % held + 1
    hit = (owner_of * cap + rank)[:, None] == jnp.arange(owner_count * cap, dtype=i32)[None, :]
    mine_table = jnp.sum(jnp.where(hit, code[:, None], 0), axis=0, dtype=i32)
    table = lax.all_gather(mine_table, "st", tiled=True)

    def swapped(first, second):
        both = jnp.concatenate([first, second], axis=1)
        return jnp.concatenate([both, lax.ppermute(both, "tp", exchange)], axis=1)

    token_weight = swapped(query_weight, gate_weight)
    row_weight = swapped(key_weight, value_weight)

    dma, vm, smem = pltpu.SemaphoreType.DMA, pltpu.VMEM, pltpu.SMEM
    rows = held * span
    qa_all, kv_all, gates = pl.pallas_call(
        functools.partial(forward_kernel, depth, plane, cap, held),
        grid_spec=pltpu.PrefetchScalarGridSpec(
            num_scalar_prefetch=1,
            in_specs=[ANY] * 7,
            out_specs=[ANY, ANY, VM],
            scratch_shapes=[
                vm((tokens, model_width), bf16), vm((rows, model_width), bf16),
                vm((model_width, width), bf16), vm((model_width, width), bf16),
                vm((model_width, width), bf16), vm((model_width, width), bf16),
                vm((tokens, width), bf16), vm((2, tokens, width), bf16),
                vm((held, span, width), bf16), vm((held, span, width), bf16),
                vm((plane, 2, slots, span, width), bf16),
                dma((6,)), dma((CHUNKS,)), dma((2,)),
                dma((depth - 1,)), dma((depth - 1,)), dma((plane - 1,)), dma((plane - 1,)),
            ],
        ),
        out_shape=[
            sds((depth, 2, tokens, width), bf16),
            sds((plane, 2, slots, span, width), bf16),
            sds((tokens, width), f32),
        ],
        compiler_params=pltpu.CompilerParams(collective_id=0, has_side_effects=True),
        name="forward",
    )(
        table, hidden, passage_store.reshape(rows, model_width),
        query_weight, gate_weight, key_weight, value_weight, output_grad,
    )
    qa_blocks = qa_all.reshape(depth, 2, block_count, block_rows, width)

    lists = [smem((plane * slots + UNROLL,), i32)] * 3
    stat = sds((2 * blocks, 2 * block_rows), f32)
    stats = pl.pallas_call(
        functools.partial(stats_kernel, sizes),
        grid_spec=pltpu.PrefetchScalarGridSpec(
            num_scalar_prefetch=1,
            in_specs=[VM] * 2,
            out_specs=VM,
            scratch_shapes=[vm((per_block, blocks, block_rows), f32)] * 3 + lists,
        ),
        out_shape=stat,
        name="stats",
    )(table, kv_all, qa_blocks)
    stats_all = pl.pallas_call(
        functools.partial(share_kernel, depth, plane),
        in_specs=[VM],
        out_specs=VM,
        out_shape=sds((depth,) + stat.shape, f32),
        scratch_shapes=[dma((depth - 1,)), dma((depth - 1,))],
        compiler_params=pltpu.CompilerParams(collective_id=1, has_side_effects=True),
        name="share",
    )(stats)
    dkv, part = pl.pallas_call(
        functools.partial(grads_kernel, sizes),
        grid_spec=pltpu.PrefetchScalarGridSpec(
            num_scalar_prefetch=1,
            in_specs=[VM] * 3,
            out_specs=[VM] * 2,
            scratch_shapes=[vm((2, blocks + 1, block_rows, width), f32)]
            + [vm((blocks, block_rows), f32)] * 3
            + lists,
        ),
        out_shape=[
            sds((plane, 2, slots, span, width), bf16),
            sds((depth, 2, block_count, block_rows, width), bf16),
        ],
        name="grads",
    )(table, kv_all, qa_blocks, stats_all)
    dkv_in, part_in = pl.pallas_call(
        functools.partial(back_kernel, depth, plane),
        in_specs=[ANY] * 2,
        out_specs=[ANY] * 2,
        out_shape=[sds(dkv.shape, bf16), sds(part.shape, bf16)],
        scratch_shapes=[
            vm(dkv.shape[1:], bf16), vm(part.shape[1:], bf16), dma((4,)),
            dma((depth - 1,)), dma((depth - 1,)), dma((plane - 1,)), dma((plane - 1,)),
        ],
        compiler_params=pltpu.CompilerParams(collective_id=2, has_side_effects=True),
        name="back",
    )(dkv, part)
    key_low, value_low = pl.pallas_call(
        functools.partial(totals_kernel, sizes),
        grid_spec=pltpu.PrefetchScalarGridSpec(
            num_scalar_prefetch=1,
            in_specs=[VM],
            out_specs=[VM] * 2,
            scratch_shapes=[vm((2, held, span, width), f32)],
        ),
        out_shape=[sds((held, span, width), bf16)] * 2,
        name="totals",
    )(table, dkv_in)

    summed = jnp.sum(part_in.astype(f32), axis=0).reshape(2, tokens, width)
    d_queries = summed[1].astype(bf16)
    s = jax.nn.sigmoid(gates)
    d_gates = (output_grad.astype(f32) * summed[0] * s * (1.0 + gates * (1.0 - s))).astype(bf16)

    def over_heads(first, second, weight):
        both = jnp.concatenate([first, second], axis=1)
        half = both.shape[0] // tp_count
        theirs = lax.dynamic_slice_in_dim(both, (tp_count - 1 - tp_index) * half, half, 0)
        mine = lax.dynamic_slice_in_dim(both, tp_index * half, half, 0)
        got = lax.ppermute(theirs, "tp", exchange)
        both = jnp.concatenate([mine, got], axis=1)
        return lax.dot_general(both, weight, NT, preferred_element_type=f32).astype(bf16)

    grad_hidden = over_heads(d_queries, d_gates, token_weight)

    store_rows = passage_store.reshape(rows, model_width)
    value_rows = value_low.reshape(rows, width)
    weight_part = lax.dot_general(store_rows, value_rows, TN, preferred_element_type=f32)
    parts = lax.all_to_all(
        weight_part.astype(bf16).reshape(owner_count, model_width // owner_count, width),
        "st", split_axis=0, concat_axis=0, tiled=True,
    )
    weight_sum = jnp.sum(parts.astype(f32), axis=0)
    shared = jnp.broadcast_to(weight_sum.astype(bf16)[None], parts.shape)
    grad_value_weight = (
        lax.all_to_all(shared, "st", split_axis=0, concat_axis=0, tiled=True)
        .reshape(model_width, width)
        .astype(f32)
    )

    grad_store = over_heads(key_low.reshape(rows, width), value_rows, row_weight).reshape(
        held // tp_count, span, model_width
    )
    return (grad_hidden, grad_store, grad_value_weight)


def solution(mesh):
    placed = (
        P("st", None),
        P("st", None, None),
        P("st", None),
        P(None, "tp"),
        P(None, "tp"),
        P(None, "tp"),
        P(None, "tp"),
        P("st", "tp"),
    )
    return jax.shard_map(
        body,
        mesh=mesh,
        in_specs=placed,
        out_specs=(P(("st", "tp"), None), P(("st", "tp"), None, None), P(None, "tp")),
        check_vma=False,
    )
```

time: 305 us -> 232 us (0.76)
  Pallas kernels: 25.2 us -> 143 us
  waiting for transfers between devices: 136 us -> 24.2 us
  blocking collectives: 53.3 us -> 14.2 us
  starting transfers between devices: 35.7 us -> 11.5 us
  matrix products: 33.1 us -> 18.6 us
    pallas_call x3 -> x6, Pallas kernels: 25.2 us -> 143 us  [the longest x1 56.6 us: body(): pl.pallas_call(functools.partial(forward_kernel, depth, plane, cap, held)...]
    all_to_all x4 -> x0, waiting for transfers between devices: 107 us -> none  [the longest x1 39.1 us: body(): lax.all_to_all(values_here[slot_passage].reshape(owner_count, capacity, s...]
    all_to_all x1 -> x0, blocking collectives: 53.3 us -> none  [totals(): lax.all_to_all(slots.reshape(owner_count, capacity, span, width), 'st', s...]
    all_to_all x4 -> x0, starting transfers between devices: 24.9 us -> none  [the longest x1 7.22 us: body(): lax.all_to_all(table.reshape(owner_count, capacity), 'st', split_axis=0,...]
    dot_general x4 -> x0, matrix products: 14.9 us -> none  [project(): return jnp.dot(rows, weight, preferred_element_type=f32)]
    unnamed x0 -> x1, blocking collectives: none -> 14.2 us
    gather x2 -> x0, local copies, waits for them, and re-layouts: 4 us -> none  [the longest x1 2 us: body(): values_here[slot_passage].reshape(owner_count, capacity, span, width)]
    concatenate x5 -> x4, other arithmetic: 8.91 us -> 8.42 us  [the longest x2 4.49 us: swapped(): both = jnp.concatenate([first, second], axis=1)]
  transfers between devices with their start and end apart: 10 -> 6, of which waited for: 8 -> 3; matrix products, arithmetic and copies ran while one was open for 16% -> 12% of each run, Pallas kernels for 4% -> 0%
where the time goes in v1:
time: 232 us
  Pallas kernels  143 us (62%)
  waiting for transfers between devices  24.2 us (10%)
  matrix products  18.6 us (8%)
  blocking collectives  14.2 us (6%)
  other arithmetic  13.4 us (6%)
  starting transfers between devices  11.5 us (5%)
  local copies, waits for them, and re-layouts  6.39 us (3%)
    pallas_call x1, Pallas kernels, body(): pl.pallas_call(functools.partial(forward_kernel, depth, plane, cap, held)...  56.6 us
    pallas_call x1, Pallas kernels, body(): pl.pallas_call(functools.partial(back_kernel, depth, plane), in_specs=[AN...  48.5 us
    pallas_call x1, Pallas kernels, body(): pl.pallas_call(functools.partial(grads_kernel, sizes), grid_spec=pltpu.Pr...  14.8 us
    all_to_all x1, waiting for transfers between devices, body(): lax.all_to_all(weight_part.astype(bf16).reshape(owner_count, model_width...  14.7 us
    unnamed x1, blocking collectives  14.2 us
    dot_general x2, matrix products, over_heads(): lax.dot_general(both, weight, NT, preferred_element_type=f32).astype(bf16)  12.5 us
    pallas_call x1, Pallas kernels, body(): pl.pallas_call(functools.partial(stats_kernel, sizes), grid_spec=pltpu.Pr...  8.81 us
    all_to_all x1, waiting for transfers between devices, body(): lax.all_to_all(shared, 'st', split_axis=0, concat_axis=0, tiled=True)  7.94 us
  transfers between devices with their start and end apart: 6, of which 3 were waited for; matrix products, arithmetic and copies ran while one was open for 12% of the time, Pallas kernels for 0%

profile of v1, /device:TPU:8, one launch (start us, length us, event | category | flops | bytes accessed | tf_op | source)
XLA Modules:
  0.0 232.3 jit_solution(16654448037837759989)
XLA Ops:
  0.6 0.8 copy.17
  1.4 0.1 reshape.134
  1.5 0.2 convert_reduce_fusion.1
  1.7 0.1 select_reduce_fusion
  1.8 1.2 dynamic-slice
  3.7 0.2 dynamic-update-slice
  3.9 14.2 %all-reduce.table = s32[1024]{0:T(1024)} all-reduce(s32[1024]{0:T(1024)S(1)} %dynamic-update-slice), channel_id=1, replica_groups=mesh['st'=16,'tp'=2] {'st'}, use_global_device_ids=true, to_apply=%add | all-reduce | flops 1024 | bytes 8192
  18.1 56.6 %forward.1 = (bf16[4,2,512,256]{3,2,1,0:T(8,128)(2,1)}, bf16[4,2,16,64,256]{4,3,2,1,0:T(8,128)(2,1)}, f32[512,256]{1,0:T(8,128)}) custom-call(s32[1024]{0:T(1024)} %all-reduce.table, bf16[512,2048]{1,0:T(8,128)(2,1)} %hidden_hbm.1, bf16[2048,2048]{1,0:T(8,128)(2,1)} %bitcast.32, bf16[2048,256]{1,0:T(8,128)(2,1)} %wq_hbm.1, bf16[2048,256]{1,0:T(8,128)(2,1)} %wg_hbm.1, ...), custom_call_target="tpu_custom_call" | custom-call | tf_op jit(solution)/shard_map/forward/pallas_call | solution.py:353
  74.7 8.8 %stats.1.own_ref = f32[64,128]{1,0:T(8,128)} custom-call(s32[1024]{0:T(1024)} %all-reduce.table, bf16[4,2,16,64,256]{4,3,2,1,0:T(8,128)(2,1)} %get-tuple-element.12.kv_ref, bf16[4,2,8,64,256]{4,3,2,1,0:T(8,128)(2,1)} %bitcast.33), custom_call_target="tpu_custom_call" | custom-call | tf_op jit(solution)/shard_map/stats/pallas_call | solution.py:385
  83.5 7.1 %share.1.stats_ref = f32[4,64,128]{2,1,0:T(8,128)} custom-call(f32[64,128]{1,0:T(8,128)} %stats.1.own_ref), custom_call_target="tpu_custom_call" | custom-call | tf_op jit(solution)/shard_map/share/pallas_call | solution.py:396
  90.6 14.8 %grads.1 = (bf16[4,2,16,64,256]{4,3,2,1,0:T(8,128)(2,1)}, bf16[4,2,8,64,256]{4,3,2,1,0:T(8,128)(2,1)}) custom-call(s32[1024]{0:T(1024)} %all-reduce.table, bf16[4,2,16,64,256]{4,3,2,1,0:T(8,128)(2,1)} %get-tuple-element.12.kv_ref, bf16[4,2,8,64,256]{4,3,2,1,0:T(8,128)(2,1)} %bitcast.34, f32[4,64,128]{2,1,0:T(8,128)} %share.1.stats_ref), custom_call_target="tpu_custom_call" | custom-call | tf_op jit(solution)/shard_map/grads/pallas_call | solution.py:405
  105.4 48.5 %back.1 = (bf16[4,2,16,64,256]{4,3,2,1,0:T(8,128)(2,1)}, bf16[4,2,8,64,256]{4,3,2,1,0:T(8,128)(2,1)}) custom-call(bf16[4,2,16,64,256]{4,3,2,1,0:T(8,128)(2,1)} %get-tuple-element.14.dkv, bf16[4,2,8,64,256]{4,3,2,1,0:T(8,128)(2,1)} %get-tuple-element.15.part), custom_call_target="tpu_custom_call" | custom-call | tf_op jit(solution)/shard_map/back/pallas_call | solution.py:421
  154.0 6.8 %totals.1 = (bf16[32,64,256]{2,1,0:T(8,128)(2,1)}, bf16[32,64,256]{2,1,0:T(8,128)(2,1)}) custom-call(s32[1024]{0:T(1024)} %all-reduce.table, bf16[4,2,16,64,256]{4,3,2,1,0:T(8,128)(2,1)} %get-tuple-element.18.dkv_ref), custom_call_target="tpu_custom_call" | custom-call | tf_op jit(solution)/shard_map/totals/pallas_call | solution.py:433
  160.8 6.1 %fusion.22 = bf16[32,16,8,128]{3,2,1,0:T(8,128)(2,1)S(1)} fusion(bf16[32,64,256]{2,1,0:T(8,128)(2,1)} %get-tuple-element.20, bf16[32,64,2048]{2,1,0:T(8,128)(2,1)} %param.9), kind=kOutput, calls=%fused_computation.26 | convolution fusion | flops 2148007936 | bytes 10485760 | tf_op jit(solution)/shard_map/dot_general | solution.py:463
  166.9 0.0 copy-start.1
  166.9 0.0 copy-start.2
  166.9 1.3 copy.24
  168.2 5.4 %all-to-all-start = ((bf16[16,128,256]{1,2,0:T(8,128)(2,1)}), bf16[16,128,256]{1,2,0:T(8,128)(2,1)}, u32[]{:S(2)}, u32[]{:S(2)}) async-start(bf16[16,128,256]{1,2,0:T(8,128)(2,1)} %bitcast.31), calls=%async_computation | async-start | bytes 2097152 | tf_op jit(solution)/shard_map/all_to_all | solution.py:464
  173.6 0.0 copy-done.1
  173.6 0.0 copy-done.2
  173.6 0.0 copy-start
  173.6 1.5 pad_maximum_fusion
  175.1 0.0 collective-permute-start.1
  175.1 3.0 %pad_maximum_fusion.1 = bf16[2048,512]{1,0:T(8,128)(2,1)} fusion(bf16[2048,256]{1,0:T(8,128)(2,1)} %wv_hbm.1, bf16[2048,256]{1,0:T(8,128)(2,1)} %wk_hbm.1), kind=kLoop, calls=%fused_computation.25 | loop fusion | flops 4194304 | bytes 4194304 | tf_op jit(solution)/shard_map/concatenate | solution.py:345
  178.1 0.5 collective-permute-start.3
  178.6 0.0 copy-start.5
  178.6 0.0 copy-done
  178.6 2.9 %fusion.24 = (bf16[1024,512]{1,0:T(8,128)(2,1)}, bf16[1024,512]{1,0:T(8,128)(2,1)}) fusion(s32[]{:T(128)S(6)} %select_n.48, bf16[2048,256]{1,0:T(8,128)(2,1)} %bitcast.36, bf16[2048,256]{1,0:T(8,128)(2,1)S(1)} %bitcast.35, s32[]{:T(128)S(6)} %select_n.49), kind=kLoop, calls=%fused_computation.28 | loop fusion | flops 4194304 | bytes 4194312 | tf_op jit(solution)/shard_map/concatenate | solution.py:451
  181.5 0.0 collective-permute-start.2
  181.6 0.0 copy-done.5
  181.6 0.0 copy-start.6
  181.6 0.4 convert_reduce_fusion
  182.0 0.8 slice.12
  182.8 0.8 slice.14
  183.6 14.7 %all-to-all-done = bf16[16,128,256]{1,2,0:T(8,128)(2,1)} async-done(((bf16[16,128,256]{1,2,0:T(8,128)(2,1)}), bf16[16,128,256]{1,2,0:T(8,128)(2,1)}, u32[]{:S(2)}, u32[]{:S(2)}) %all-to-all-start) | async-done | bytes 1048608 | tf_op jit(solution)/shard_map/all_to_all | solution.py:464
  198.2 1.4 reduce_sum.42
  199.6 0.1 copy.20
  199.7 1.1 broadcast_in_dim.16
  200.8 5.5 %all-to-all-start.1 = ((bf16[16,128,256]{2,1,0:T(8,128)(2,1)}), bf16[16,128,256]{2,1,0:T(8,128)(2,1)S(1)}, u32[]{:S(2)}, u32[]{:S(2)}) async-start(bf16[16,128,256]{2,1,0:T(8,128)(2,1)} %broadcast_in_dim.16), calls=%async_computation.1 | async-start | bytes 2097152 | tf_op jit(solution)/shard_map/all_to_all | solution.py:471
  206.3 0.0 copy-done.6
  206.3 1.4 fusion.30
  207.7 1.0 fusion.32
  208.7 0.1 collective-permute-start
  208.8 1.5 collective-permute-done
  210.3 0.0 collective-permute-done.1
  210.3 0.0 copy-start.3
  210.3 0.0 copy-start.4
  210.3 0.0 copy-start.7
  210.3 4.0 %fusion.15 = bf16[256,2048]{1,0:T(8,128)(2,1)} fusion(bf16[2048,512]{1,0:T(8,128)(2,1)} %collective-permute-done.1, bf16[2048,256]{1,0:T(8,128)(2,1)S(1)} %copy-done.1, bf16[2048,256]{1,0:T(8,128)(2,1)S(1)} %copy-done.2, bf16[256,512]{1,0:T(8,128)(2,1)S(1)} %collective-permute-done, bf16[256,512]{1,0:T(8,128)(2,1)S(1)} %get-tuple-element.23), kind=kOutput, calls=%fused_computation.15 | convolution fusion | flops 1087897600 | bytes 5767168 | tf_op jit(solution)/shard_map/dot_general | solution.py:457
  214.4 0.0 collective-permute-done.2
  214.4 0.0 collective-permute-done.3
  214.4 0.0 copy-done.3
  214.4 0.0 copy-done.4
  214.4 0.0 copy-done.7
  214.4 8.5 %fusion.12 = bf16[1024,2048]{1,0:T(8,128)(2,1)} fusion(bf16[2048,512]{1,0:T(8,128)(2,1)} %collective-permute-done.3, bf16[2048,256]{1,0:T(8,128)(2,1)S(1)} %copy-done.4, bf16[2048,256]{1,0:T(8,128)(2,1)S(1)} %copy-done.3, bf16[1024,512]{1,0:T(8,128)(2,1)} %collective-permute-done.2, bf16[1024,512]{1,0:T(8,128)(2,1)S(1)} %copy-done.7), kind=kOutput, calls=%fused_computation.13 | convolution fusion | flops 4313841664 | bytes 10485760 | tf_op jit(solution)/shard_map/dot_general | solution.py:457
  222.9 7.9 %all-to-all-done.1 = bf16[16,128,256]{2,1,0:T(8,128)(2,1)S(1)} async-done(((bf16[16,128,256]{2,1,0:T(8,128)(2,1)}), bf16[16,128,256]{2,1,0:T(8,128)(2,1)S(1)}, u32[]{:S(2)}, u32[]{:S(2)}) %all-to-all-start.1) | async-done | bytes 1048608 | tf_op jit(solution)/shard_map/all_to_all | solution.py:471
  230.8 1.5 bitcast_convert_fusion
  (3 shorter events, 0.0 us)
Async XLA Ops:
  166.9 6.7 %copy-start.1 = (bf16[2048,256]{1,0:T(8,128)(2,1)S(1)}, bf16[2048,256]{1,0:T(8,128)(2,1)}, u32[]{:S(2)}) copy-start(bf16[2048,256]{1,0:T(8,128)(2,1)} %wg_hbm.1) | copy-start | bytes 3145732
  166.9 6.7 %copy-start.2 = (bf16[2048,256]{1,0:T(8,128)(2,1)S(1)}, bf16[2048,256]{1,0:T(8,128)(2,1)}, u32[]{:S(2)}) copy-start(bf16[2048,256]{1,0:T(8,128)(2,1)} %wq_hbm.1) | copy-start | bytes 3145732
  168.2 30.1 %all-to-all-start = ((bf16[16,128,256]{1,2,0:T(8,128)(2,1)}), bf16[16,128,256]{1,2,0:T(8,128)(2,1)}, u32[]{:S(2)}, u32[]{:S(2)}) async-start(bf16[16,128,256]{1,2,0:T(8,128)(2,1)} %bitcast.31), calls=%async_computation | async-start | bytes 2097152 | tf_op jit(solution)/shard_map/all_to_all | solution.py:464
  173.6 5.0 %copy-start = (bf16[32,64,256]{2,1,0:T(8,128)(2,1)S(1)}, bf16[32,64,256]{2,1,0:T(8,128)(2,1)}, u32[]{:S(2)}) copy-start(bf16[32,64,256]{2,1,0:T(8,128)(2,1)} %get-tuple-element.20) | copy-start | bytes 3145732
  175.1 35.2 %collective-permute-start.1 = (bf16[2048,512]{1,0:T(8,128)(2,1)}, bf16[2048,512]{1,0:T(8,128)(2,1)}, u32[]{:S(2)}, u32[]{:S(2)}) collective-permute-start(bf16[2048,512]{1,0:T(8,128)(2,1)} %pad_maximum_fusion), channel_id=1, source_target_pairs={{0,1},{1,0},{2,3},{3,2},{4,5},{5,4},{6,7},{7,6},{8,9},{9,8},{10,11... | collective-permute-start | bytes 6291464 | tf_op jit(solution)/shard_map/ppermute | solution.py:346
  178.1 36.2 %collective-permute-start.3 = (bf16[2048,512]{1,0:T(8,128)(2,1)}, bf16[2048,512]{1,0:T(8,128)(2,1)}, u32[]{:S(2)}, u32[]{:S(2)}) collective-permute-start(bf16[2048,512]{1,0:T(8,128)(2,1)} %pad_maximum_fusion.1), channel_id=1, source_target_pairs={{0,1},{1,0},{2,3},{3,2},{4,5},{5,4},{6,7},{7,6},{8,9},{9,8},{10,11... | collective-permute-start | bytes 6291464 | tf_op jit(solution)/shard_map/ppermute | solution.py:346
  178.6 2.9 %copy-start.5 = (bf16[4,2,8,64,256]{4,3,2,1,0:T(8,128)(2,1)S(1)}, bf16[4,2,8,64,256]{4,3,2,1,0:T(8,128)(2,1)}, u32[]{:S(2)}) copy-start(bf16[4,2,8,64,256]{4,3,2,1,0:T(8,128)(2,1)} %get-tuple-element.16) | copy-start | bytes 6291460
  181.5 32.8 %collective-permute-start.2 = (bf16[1024,512]{1,0:T(8,128)(2,1)}, bf16[1024,512]{1,0:T(8,128)(2,1)}, u32[]{:S(2)}, u32[]{:S(2)}) collective-permute-start(bf16[1024,512]{1,0:T(8,128)(2,1)} %get-tuple-element.22), channel_id=1, source_target_pairs={{0,1},{1,0},{2,3},{3,2},{4,5},{5,4},{6,7},{7,6},{8,9},{9,8},{10,11... | collective-permute-start | bytes 3145736 | tf_op jit(solution)/shard_map/ppermute | solution.py:455
  181.6 24.7 %copy-start.6 = (bf16[512,256]{1,0:T(8,128)(2,1)S(1)}, bf16[512,256]{1,0:T(8,128)(2,1)}, u32[]{:S(2)}) copy-start(bf16[512,256]{1,0:T(8,128)(2,1)} %up_hbm.1) | copy-start | bytes 786436
  200.8 30.0 %all-to-all-start.1 = ((bf16[16,128,256]{2,1,0:T(8,128)(2,1)}), bf16[16,128,256]{2,1,0:T(8,128)(2,1)S(1)}, u32[]{:S(2)}, u32[]{:S(2)}) async-start(bf16[16,128,256]{2,1,0:T(8,128)(2,1)} %broadcast_in_dim.16), calls=%async_computation.1 | async-start | bytes 2097152 | tf_op jit(solution)/shard_map/all_to_all | solution.py:471
  208.7 1.6 collective-permute-start
  210.3 4.1 %copy-start.3 = (bf16[2048,256]{1,0:T(8,128)(2,1)S(1)}, bf16[2048,256]{1,0:T(8,128)(2,1)}, u32[]{:S(2)}) copy-start(bf16[2048,256]{1,0:T(8,128)(2,1)} %wk_hbm.1) | copy-start | bytes 3145732
  210.3 4.1 %copy-start.4 = (bf16[2048,256]{1,0:T(8,128)(2,1)S(1)}, bf16[2048,256]{1,0:T(8,128)(2,1)}, u32[]{:S(2)}) copy-start(bf16[2048,256]{1,0:T(8,128)(2,1)} %wv_hbm.1) | copy-start | bytes 3145732
  210.3 4.1 %copy-start.7 = (bf16[1024,512]{1,0:T(8,128)(2,1)S(1)}, bf16[1024,512]{1,0:T(8,128)(2,1)}, u32[]{:S(2)}) copy-start(bf16[1024,512]{1,0:T(8,128)(2,1)} %get-tuple-element.21) | copy-start | bytes 3145732

commit v2 on v0

v2 whole, which is shorter than its diff:
```python
import functools
import math

import jax
import jax.numpy as jnp
from jax import lax
from jax.experimental import pallas as pl
from jax.experimental.pallas import tpu as pltpu
from jax.sharding import PartitionSpec as P

HEAD_DIM = 256
NT = (((1,), (1,)), ((), ()))
TN = (((0,), (0,)), ((), ()))
MESH = pl.DeviceIdType.MESH
UNROLL = 4
CHUNKS = 8
LOW = -1e30
bf16, f32, i32 = jnp.bfloat16, jnp.float32, jnp.int32
ANY = pl.BlockSpec(memory_space=pl.ANY)
VM = pl.BlockSpec(memory_space=pltpu.VMEM)


def greet(peers):
    barrier = pltpu.get_barrier_semaphore()
    for peer in peers:
        pl.semaphore_signal(barrier, inc=1, device_id={"st": peer}, device_id_type=MESH)
    pl.semaphore_wait(barrier, len(peers))


def place(depth, plane):
    me = lax.axis_index("st")
    my_z, my_p = me // plane, me % plane
    column = [((my_z + d) % depth) * plane + my_p for d in range(1, depth)]
    row = [my_z * plane + (my_p + d) % plane for d in range(1, plane)]
    return me, my_z, my_p, column, row


def remote(src, dst, send, recv, peer):
    return pltpu.make_async_remote_copy(
        src_ref=src, dst_ref=dst, send_sem=send, recv_sem=recv,
        device_id={"st": peer}, device_id_type=MESH,
    )


def core_kernel(
    sizes, mine, hidden_hbm, store_hbm, wq_hbm, wg_hbm, wk_hbm, wv_hbm, up_hbm,
    tab_out, gate_ref, dk_in, dv_in, part_in,
    hidden, store, wq, wg, wk, wv, up, q_all, da_all, keys, values, pack_k, pack_v, k_in, v_in,
    score_at, dprob_at, dk_out, dv_out, piece, part_out,
    tops, sums, mids, marks, block_top, block_sum, block_mid, stat_own, stat_all, tab_v, tab,
    load_sem, chunk_sem, own_sem, tab_sem, tsend, trecv, qsend, qrecv, asend, arecv, ksend, krecv, vsend, vrecv,
    ssend, srecv, gksend, gkrecv, gvsend, gvrecv, psend, precv,
):
    depth, plane, cap, held, requests, per_block = sizes
    me, my_z, my_p, column, row = place(depth, plane)
    owners, slots, mixed = depth * plane, depth * cap, plane * cap
    per_reader = requests // per_block
    rows = store.shape[0] // CHUNKS
    span, width = keys.shape[1:]
    passages = rows // span
    scale = HEAD_DIM ** (-0.5)
    loads = [
        pltpu.make_async_copy(a, b, load_sem.at[i])
        for i, (a, b) in enumerate(
            ((hidden_hbm, hidden), (wq_hbm, wq), (wg_hbm, wg), (up_hbm, up), (wk_hbm, wk), (wv_hbm, wv))
        )
    ]
    for c in loads[:5]:
        c.start()

    def chunk(c):
        at = pl.ds(pl.multiple_of(c * rows, rows), rows)
        return pltpu.make_async_copy(store_hbm.at[at], store.at[at], chunk_sem.at[c])

    for c in range(CHUNKS):
        chunk(c).start()
    loads[5].start()
    tab_v[me] = mine[...]

    barrier = pltpu.get_barrier_semaphore()

    @pl.loop(1, owners)
    def _(d):
        pl.semaphore_signal(barrier, inc=1, device_id={"st": (me + d) % owners}, device_id_type=MESH)

    pl.semaphore_wait(barrier, owners - 1)

    def table_copy(d):
        return remote(mine, tab_v.at[me], tsend.at[d - 1], trecv.at[d - 1], (me + d) % owners)

    @pl.loop(1, owners)
    def _(d):
        table_copy(d).start()

    loads[0].wait()
    loads[1].wait()
    tiles = q_all.shape[1:]
    q_all[my_z] = jnp.dot(hidden[...], wq[...], preferred_element_type=f32).astype(bf16).reshape(tiles)
    q_copies = [remote(q_all.at[my_z], q_all.at[my_z], qsend.at[i], qrecv.at[i], p) for i, p in enumerate(column)]
    for c in q_copies:
        c.start()
    loads[2].wait()
    loads[3].wait()
    gates = jnp.dot(hidden[...], wg[...], preferred_element_type=f32)
    gate_ref[...] = gates
    da_all[my_z] = (up[...].astype(f32) * gates * jax.nn.sigmoid(gates)).astype(bf16).reshape(tiles)
    a_copies = [remote(da_all.at[my_z], da_all.at[my_z], asend.at[i], arecv.at[i], p) for i, p in enumerate(column)]
    for c in a_copies:
        c.start()

    def project(weight, out, fetch):
        @pl.loop(0, CHUNKS)
        def _(c):
            if fetch:
                chunk(c).wait()
            part = store[pl.ds(pl.multiple_of(c * rows, rows), rows)]
            out[pl.ds(c * passages, passages)] = jnp.dot(
                part, weight[...], preferred_element_type=f32
            ).astype(bf16).reshape(passages, span, width)

    def spread(source, pack, landed, send, recv):
        copies = []
        for i in range(plane):
            own = i == plane - 1
            peer_p = my_p if own else row[i] % plane

            @pl.loop(0, slots)
            def _(s):
                code = tab[(s // cap) * plane + peer_p, 0, me * cap + s % cap]
                value = source[jnp.maximum(code - 1, 0) % held]
                if own:
                    landed[my_p, s] = value
                else:
                    pack[i, s] = value

            if not own:
                copies.append(remote(pack.at[i], landed.at[my_p], send.at[i], recv.at[i], row[i]))
                copies[-1].start()
        return copies

    loads[4].wait()
    project(wk, keys, True)

    @pl.loop(1, owners)
    def _(d):
        table_copy(d).wait()

    to_smem = pltpu.make_async_copy(tab_v, tab, tab_sem.at[0])
    to_out = pltpu.make_async_copy(tab_v, tab_out, tab_sem.at[1])
    to_smem.start()
    to_out.start()
    to_smem.wait()
    k_copies = spread(keys, pack_k, k_in, ksend, krecv)
    loads[5].wait()
    project(wv, values, False)
    v_copies = spread(values, pack_v, v_in, vsend, vrecv)

    def code_of(z, p, c):
        return tab[z * plane + my_p, 0, (my_z * plane + p) * cap + c]

    def block_of(code):
        return (jnp.maximum(code - 1, 0) // held) // per_block

    for c in q_copies:
        c.wait()
    for i in range(plane):
        src = my_p if i == 0 else (my_p + plane - i) % plane
        if i:
            k_copies[i - 1].wait()

        @pl.loop(0, slots // UNROLL)
        def _(t):
            for u in range(UNROLL):
                zc = t * UNROLL + u
                z, c = zc // cap, zc % cap
                q = q_all[z, block_of(code_of(z, src, c))]
                score_at[src, zc] = lax.dot_general(k_in[src, zc], q, NT, preferred_element_type=f32) * scale

    for c in a_copies:
        c.wait()
    for i in range(plane):
        src = my_p if i == 0 else (my_p + plane - i) % plane
        if i:
            v_copies[i - 1].wait()

        @pl.loop(0, slots // UNROLL)
        def _(t):
            for u in range(UNROLL):
                zc = t * UNROLL + u
                z, c = zc // cap, zc % cap
                code = code_of(z, src, c)
                block = block_of(code)
                d_probs = lax.dot_general(v_in[src, zc], da_all[z, block], NT, preferred_element_type=f32)
                dprob_at[src, zc] = d_probs
                scores = score_at[src, zc]
                top = jnp.max(scores, axis=0, keepdims=True)
                e = jnp.exp(scores - top)
                at = pl.ds(z * mixed + src * cap + c, 1)
                tops[at, :] = top
                sums[at, :] = jnp.sum(e, axis=0, keepdims=True)
                mids[at, :] = jnp.sum(e * d_probs, axis=0, keepdims=True)
                marks[at, :] = jnp.full(top.shape, jnp.where(code > 0, block, -1), i32)

    blocks = depth * per_reader
    for z in range(depth):
        at = slice(z * mixed, (z + 1) * mixed)
        m, l, c, mark = tops[at], sums[at], mids[at], marks[at]
        for b in range(per_reader):
            on = mark == b
            top = jnp.max(jnp.where(on, m, LOW), axis=0, keepdims=True)
            ratio = jnp.where(on, jnp.exp(jnp.minimum(m - top, 0.0)), 0.0)
            to = slice(z * per_reader + b, z * per_reader + b + 1)
            block_top[to, :] = top
            block_sum[to, :] = jnp.sum(l * ratio, axis=0, keepdims=True)
            block_mid[to, :] = jnp.sum(c * ratio, axis=0, keepdims=True)
    stat_own[0:blocks] = jnp.concatenate([block_top[...], block_sum[...]], axis=1)
    stat_own[blocks:] = jnp.concatenate([block_mid[...], block_mid[...]], axis=1)
    s_copies = [remote(stat_own, stat_all.at[my_z], ssend.at[i], srecv.at[i], p) for i, p in enumerate(column)]
    for c in s_copies:
        c.start()
    stat_all[my_z] = stat_own[...]
    for i in range(2):
        piece[mixed, i] = jnp.zeros(piece.shape[2:], f32)
    for c in s_copies:
        c.wait()
    heads = [stat_all[z, 0:blocks, 0:span] for z in range(depth)]
    top = functools.reduce(jnp.maximum, heads)
    ratios = [jnp.exp(h - top) for h in heads]
    total = sum(stat_all[z, 0:blocks, span:] * ratios[z] for z in range(depth))
    mid = sum(stat_all[z, blocks:, 0:span] * ratios[z] for z in range(depth))
    inverse = 1.0 / total
    block_top[...] = top
    block_sum[...] = inverse
    block_mid[...] = mid * inverse

    back = []
    for d in range(1, depth + 1):
        z = (my_z + d) % depth

        @pl.loop(0, mixed // UNROLL)
        def _(t):
            for u in range(UNROLL):
                idx = t * UNROLL + u
                p, c = idx // cap, idx % cap
                zc = z * cap + c
                code = code_of(z, p, c)
                block = block_of(code)
                at = pl.ds(z * per_reader + block, 1)
                top = jnp.where(code > 0, block_top[at, :], -LOW)
                probs = jnp.exp(score_at[p, zc] - top) * block_sum[at, :]
                low = probs.astype(bf16)
                d_scores = (probs * (dprob_at[p, zc] - block_mid[at, :]) * scale).astype(bf16)
                dk_out[p, zc] = jnp.dot(d_scores, q_all[z, block], preferred_element_type=f32).astype(bf16)
                dv_out[p, zc] = jnp.dot(low, da_all[z, block], preferred_element_type=f32).astype(bf16)
                piece[idx, 0] = lax.dot_general(low, v_in[p, zc], TN, preferred_element_type=f32)
                piece[idx, 1] = lax.dot_general(d_scores, k_in[p, zc], TN, preferred_element_type=f32)

        @pl.loop(0, per_reader)
        def _(b):
            found = []
            for j in range(per_block):
                flat = tab[z * plane + my_p, 0, owners * cap + b * per_block + j]
                near = flat // mixed == my_z
                found.append(jnp.where(near, flat % mixed, mixed))
            for i in range(2):
                part_out[z, i, b] = sum(piece[f, i] for f in found).astype(bf16)

        at = pl.ds(z * cap, cap)
        if d < depth:
            back.append(remote(part_out.at[z], part_in.at[my_z], psend.at[d - 1], precv.at[d - 1], column[d - 1]))
        else:
            back.append(pltpu.make_async_copy(part_out.at[z], part_in.at[my_z], own_sem.at[0]))
        back[-1].start()
        for i, peer in enumerate(row):
            p = peer % plane
            n = (d - 1) * (plane - 1) + i
            for out, into, send, recv in ((dv_out, dv_in, gvsend, gvrecv), (dk_out, dk_in, gksend, gkrecv)):
                back.append(remote(out.at[p, at], into.at[my_p, at], send.at[n], recv.at[n], peer))
                back[-1].start()
    for i, (out, into) in enumerate(((dv_out, dv_in), (dk_out, dk_in))):
        back.append(pltpu.make_async_copy(out.at[my_p], into.at[my_p], own_sem.at[1 + i]))
        back[-1].start()
    to_out.wait()
    for c in back:
        c.wait()


def totals_kernel(sizes, table, dk_ref, dv_ref, key_ref, value_ref, acc):
    depth, plane, cap, held, _, _ = sizes
    slots = depth * cap
    me = lax.axis_index("st")
    acc[...] = jnp.zeros_like(acc)

    @pl.loop(0, plane * slots)
    def _(s):
        p, zc = s // slots, s % slots
        code = table[(zc // cap) * plane + p, 0, me * cap + zc % cap]

        @pl.when(code > 0)
        def _():
            at = (code - 1) % held
            acc[0, at] += dk_ref[p, zc].astype(f32)
            acc[1, at] += dv_ref[p, zc].astype(f32)

    key_ref[...] = acc[0].astype(bf16)
    value_ref[...] = acc[1].astype(bf16)


def body(
    hidden,
    passage_store,
    passage_ids,
    query_weight,
    gate_weight,
    key_weight,
    value_weight,
    output_grad,
):
    owner_count = lax.axis_size("st")
    tp_count = lax.axis_size("tp")
    tp_index = lax.axis_index("tp")
    depth = 2 ** ((int(math.log2(owner_count)) + 1) // 2)
    plane = owner_count // depth
    held, span, model_width = passage_store.shape
    block_count, per_block = passage_ids.shape
    requests = block_count * per_block
    cap = max(1, 2 * requests // owner_count)
    width = query_weight.shape[1]
    tokens = hidden.shape[0]
    block_rows = tokens // block_count
    slots, mixed = depth * cap, plane * cap
    blocks = depth * block_count
    sizes = (depth, plane, cap, held, requests, per_block)
    exchange = [(i, tp_count - 1 - i) for i in range(tp_count)]
    sds = jax.ShapeDtypeStruct

    ids = passage_ids.reshape(requests)
    owner_of = ids // held
    positions = jnp.arange(requests, dtype=i32)
    earlier = positions[None, :] < positions[:, None]
    rank = jnp.sum((owner_of[:, None] == owner_of[None, :]) & earlier, axis=1, dtype=i32)
    code = positions * held + ids % held + 1
    hit = (owner_of * cap + rank)[:, None] == jnp.arange(owner_count * cap, dtype=i32)[None, :]
    slot_codes = jnp.sum(jnp.where(hit, code[:, None], 0), axis=0, dtype=i32)
    lanes, entries = 128, owner_count * cap + requests
    words = -(-entries // lanes) * lanes
    mine_table = jnp.pad(jnp.concatenate([slot_codes, owner_of * cap + rank]), (0, 8 * words - entries)).reshape(8, words)

    def swapped(first, second):
        both = jnp.concatenate([first, second], axis=1)
        return jnp.concatenate([both, lax.ppermute(both, "tp", exchange)], axis=1)

    token_weight = swapped(query_weight, gate_weight)
    row_weight = swapped(key_weight, value_weight)

    dma, vm, smem = pltpu.SemaphoreType.DMA, pltpu.VMEM, pltpu.SMEM
    rows = held * span
    slot_block = vm((plane, slots, span, width), bf16)
    near = dma((plane - 1,))
    far = dma((depth - 1,))
    each = dma((depth * (plane - 1),))
    stat = vm((depth * mixed, block_rows), f32)
    table, gates, dk_in, dv_in, part_in = pl.pallas_call(
        functools.partial(core_kernel, sizes),
        in_specs=[VM] + [ANY] * 7,
        out_specs=[ANY, VM, ANY, ANY, ANY],
        out_shape=[
            sds((owner_count,) + mine_table.shape, i32),
            sds((tokens, width), f32),
            sds((plane, slots, span, width), bf16),
            sds((plane, slots, span, width), bf16),
            sds((depth, 2, block_count, block_rows, width), bf16),
        ],
        scratch_shapes=[
            vm((tokens, model_width), bf16), vm((rows, model_width), bf16),
            *[vm((model_width, width), bf16)] * 4,
            vm((tokens, width), bf16),
            *[vm((depth, block_count, block_rows, width), bf16)] * 2,
            *[vm((held, span, width), bf16)] * 2,
            *[vm((plane - 1, slots, span, width), bf16)] * 2,
            slot_block, slot_block,
            *[vm((plane, slots, span, block_rows), f32)] * 2,
            slot_block, slot_block,
            vm((mixed + 1, 2, block_rows, width), f32),
            vm((depth, 2, block_count, block_rows, width), bf16),
            stat, stat, stat, vm((depth * mixed, block_rows), i32),
            *[vm((blocks, block_rows), f32)] * 3,
            vm((2 * blocks, 2 * block_rows), f32), vm((depth, 2 * blocks, 2 * block_rows), f32),
            vm((owner_count,) + mine_table.shape, i32), smem((owner_count,) + mine_table.shape, i32),
            dma((6,)), dma((CHUNKS,)), dma((3,)), dma((2,)),
            dma((owner_count - 1,)), dma((owner_count - 1,)),
            far, far, far, far, near, near, near, near, far, far, each, each, each, each, far, far,
        ],
        compiler_params=pltpu.CompilerParams(collective_id=0, has_side_effects=True, vmem_limit_bytes=63 << 20),
        name="core",
    )(
        mine_table, hidden, passage_store.reshape(rows, model_width),
        query_weight, gate_weight, key_weight, value_weight, output_grad,
    )
    key_low, value_low = pl.pallas_call(
        functools.partial(totals_kernel, sizes),
        in_specs=[pl.BlockSpec(memory_space=smem), VM, VM],
        out_specs=[VM] * 2,
        scratch_shapes=[vm((2, held, span, width), f32)],
        out_shape=[sds((held, span, width), bf16)] * 2,
        name="totals",
    )(table, dk_in, dv_in)

    summed = jnp.sum(part_in.astype(f32), axis=0).reshape(2, tokens, width)
    d_queries = summed[1].astype(bf16)
    s = jax.nn.sigmoid(gates)
    d_gates = (output_grad.astype(f32) * summed[0] * s * (1.0 + gates * (1.0 - s))).astype(bf16)

    def over_heads(first, second, weight):
        both = jnp.concatenate([first, second], axis=1)
        half = both.shape[0] // tp_count
        theirs = lax.dynamic_slice_in_dim(both, (tp_count - 1 - tp_index) * half, half, 0)
        mine = lax.dynamic_slice_in_dim(both, tp_index * half, half, 0)
        got = lax.ppermute(theirs, "tp", exchange)
        both = jnp.concatenate([mine, got], axis=1)
        return lax.dot_general(both, weight, NT, preferred_element_type=f32).astype(bf16)

    grad_hidden = over_heads(d_queries, d_gates, token_weight)

    store_rows = passage_store.reshape(rows, model_width)
    value_rows = value_low.reshape(rows, width)
    weight_part = lax.dot_general(store_rows, value_rows, TN, preferred_element_type=f32)
    parts = lax.all_to_all(
        weight_part.astype(bf16).reshape(owner_count, model_width // owner_count, width),
        "st", split_axis=0, concat_axis=0, tiled=True,
    )
    weight_sum = jnp.sum(parts.astype(f32), axis=0)
    shared = jnp.broadcast_to(weight_sum.astype(bf16)[None], parts.shape)
    grad_value_weight = (
        lax.all_to_all(shared, "st", split_axis=0, concat_axis=0, tiled=True)
        .reshape(model_width, width)
        .astype(f32)
    )

    grad_store = over_heads(key_low.reshape(rows, width), value_rows, row_weight).reshape(
        held // tp_count, span, model_width
    )
    return (grad_hidden, grad_store, grad_value_weight)


def solution(mesh):
    placed = (
        P("st", None),
        P("st", None, None),
        P("st", None),
        P(None, "tp"),
        P(None, "tp"),
        P(None, "tp"),
        P(None, "tp"),
        P("st", "tp"),
    )
    return jax.shard_map(
        body,
        mesh=mesh,
        in_specs=placed,
        out_specs=(P(("st", "tp"), None), P(("st", "tp"), None, None), P(None, "tp")),
        check_vma=False,
    )
```

time: 305 us -> 197 us (0.65)
  waiting for transfers between devices: 136 us -> 24.3 us
  Pallas kernels: 25.2 us -> 123 us
  blocking collectives: 53.3 us -> 0 us
  starting transfers between devices: 35.7 us -> 10.7 us
  matrix products: 33.1 us -> 18.6 us
  local copies, waits for them, and re-layouts: 9.17 us -> 5.49 us
    all_to_all x4 -> x0, waiting for transfers between devices: 107 us -> none  [the longest x1 39.1 us: body(): lax.all_to_all(values_here[slot_passage].reshape(owner_count, capacity, s...]
    pallas_call x3 -> x2, Pallas kernels: 25.2 us -> 123 us  [the longest x1 117 us: body(): pl.pallas_call(functools.partial(core_kernel, sizes), in_specs=[VM] + [AN...]
    all_to_all x1 -> x0, blocking collectives: 53.3 us -> none  [totals(): lax.all_to_all(slots.reshape(owner_count, capacity, span, width), 'st', s...]
    all_to_all x4 -> x0, starting transfers between devices: 24.9 us -> none  [the longest x1 7.22 us: body(): lax.all_to_all(table.reshape(owner_count, capacity), 'st', split_axis=0,...]
    dot_general x4 -> x0, matrix products: 14.9 us -> none  [project(): return jnp.dot(rows, weight, preferred_element_type=f32)]
    gather x2 -> x0, local copies, waits for them, and re-layouts: 4 us -> none  [the longest x1 2 us: body(): values_here[slot_passage].reshape(owner_count, capacity, span, width)]
  transfers between devices with their start and end apart: 10 -> 6, of which waited for: 8 -> 3; matrix products, arithmetic and copies ran while one was open for 16% -> 14% of each run, Pallas kernels for 4% -> 0%
where the time goes in v2:
time: 197 us
  Pallas kernels  123 us (62%)
  waiting for transfers between devices  24.3 us (12%)
  matrix products  18.6 us (9%)
  other arithmetic  13.5 us (7%)
  starting transfers between devices  10.7 us (5%)
  local copies, waits for them, and re-layouts  5.49 us (3%)
    pallas_call x1, Pallas kernels, body(): pl.pallas_call(functools.partial(core_kernel, sizes), in_specs=[VM] + [AN...  117 us
    all_to_all x1, waiting for transfers between devices, body(): lax.all_to_all(weight_part.astype(bf16).reshape(owner_count, model_width...  15.1 us
    dot_general x2, matrix products, over_heads(): lax.dot_general(both, weight, NT, preferred_element_type=f32).astype(bf16)  12.5 us
    all_to_all x1, waiting for transfers between devices, body(): lax.all_to_all(shared, 'st', split_axis=0, concat_axis=0, tiled=True)  7.61 us
    pallas_call x1, Pallas kernels, body(): pl.pallas_call(functools.partial(totals_kernel, sizes), in_specs=[pl.Bloc...  6.17 us
    dot_general x1, matrix products, body(): lax.dot_general(store_rows, value_rows, TN, preferred_element_type=f32)  6.06 us
    all_to_all x1, starting transfers between devices, body(): lax.all_to_all(weight_part.astype(bf16).reshape(owner_count, model_width...  5.28 us
    all_to_all x1, starting transfers between devices, body(): lax.all_to_all(shared, 'st', split_axis=0, concat_axis=0, tiled=True)  4.84 us
  transfers between devices with their start and end apart: 6, of which 3 were waited for; matrix products, arithmetic and copies ran while one was open for 14% of the time, Pallas kernels for 0%

profile of v2, /device:TPU:8, one launch (start us, length us, event | category | flops | bytes accessed | tf_op | source)
XLA Modules:
  0.0 196.6 jit_solution(18441728665032457000)
XLA Ops:
  0.6 0.8 copy.17
  1.4 0.1 reshape.134
  1.5 0.2 convert_reduce_fusion.1
  1.7 0.1 select_reduce_fusion
  1.8 0.1 pad_add_fusion
  1.8 0.6 pad_bitcast_fusion.mine
  2.5 117.1 %core.1 = (s32[16,8,128]{2,1,0:T(8,128)}, f32[512,256]{1,0:T(8,128)}, bf16[4,16,64,256]{3,2,1,0:T(8,128)(2,1)}, bf16[4,16,64,256]{3,2,1,0:T(8,128)(2,1)}, bf16[4,2,8,64,256]{4,3,2,1,0:T(8,128)(2,1)}) custom-call(s32[8,128]{1,0:T(8,128)} %pad_bitcast_fusion.mine, bf16[512,2048]{1,0:T(8,128)(2,1)} %hidden_hbm.1, bf16[2048,2048]{1,0:T(8,128)(2,1)} %bitcast.32, ...), custom_call_target="tpu_custom_call" | custom-call | tf_op jit(solution)/shard_map/core/pallas_call | solution.py:363
  119.6 6.2 %totals.1 = (bf16[32,64,256]{2,1,0:T(8,128)(2,1)}, bf16[32,64,256]{2,1,0:T(8,128)(2,1)}) custom-call(s32[16,8,128]{2,1,0:T(8,128)} %get-tuple-element.12.table, bf16[4,16,64,256]{3,2,1,0:T(8,128)(2,1)} %get-tuple-element.13.dk_ref, bf16[4,16,64,256]{3,2,1,0:T(8,128)(2,1)} %get-tuple-element.14.dv_ref), custom_call_target="tpu_custom_call" | custom-call | tf_op jit(solution)/shard_map/totals/pallas_call | solution.py:400
  125.7 6.1 %fusion.22 = bf16[32,16,8,128]{3,2,1,0:T(8,128)(2,1)S(1)} fusion(bf16[32,64,256]{2,1,0:T(8,128)(2,1)} %get-tuple-element.16, bf16[32,64,2048]{2,1,0:T(8,128)(2,1)} %param.9), kind=kOutput, calls=%fused_computation.26 | convolution fusion | flops 2148007936 | bytes 10485760 | tf_op jit(solution)/shard_map/dot_general | solution.py:427
  131.8 0.0 copy-start.1
  131.8 0.0 copy-start.2
  131.8 1.2 copy.24
  133.1 5.3 %all-to-all-start = ((bf16[16,128,256]{1,2,0:T(8,128)(2,1)}), bf16[16,128,256]{1,2,0:T(8,128)(2,1)}, u32[]{:S(2)}, u32[]{:S(2)}) async-start(bf16[16,128,256]{1,2,0:T(8,128)(2,1)} %bitcast.31), calls=%async_computation | async-start | bytes 2097152 | tf_op jit(solution)/shard_map/all_to_all | solution.py:428
  138.4 0.0 copy-done.1
  138.4 0.0 copy-done.2
  138.4 0.0 copy-start
  138.4 1.5 pad_maximum_fusion
  139.9 0.0 collective-permute-start.1
  139.9 3.0 %pad_maximum_fusion.1 = bf16[2048,512]{1,0:T(8,128)(2,1)} fusion(bf16[2048,256]{1,0:T(8,128)(2,1)} %wv_hbm.1, bf16[2048,256]{1,0:T(8,128)(2,1)} %wk_hbm.1), kind=kLoop, calls=%fused_computation.25 | loop fusion | flops 4194304 | bytes 4194304 | tf_op jit(solution)/shard_map/concatenate | solution.py:350
  142.9 0.5 collective-permute-start.3
  143.4 0.0 copy-start.5
  143.4 0.0 copy-done
  143.4 2.9 %fusion.24 = (bf16[1024,512]{1,0:T(8,128)(2,1)}, bf16[1024,512]{1,0:T(8,128)(2,1)}) fusion(s32[]{:T(128)S(6)} %select_n.48, bf16[2048,256]{1,0:T(8,128)(2,1)} %bitcast.34, bf16[2048,256]{1,0:T(8,128)(2,1)S(1)} %bitcast.33, s32[]{:T(128)S(6)} %select_n.49), kind=kLoop, calls=%fused_computation.28 | loop fusion | flops 4194304 | bytes 4194312 | tf_op jit(solution)/shard_map/concatenate | solution.py:415
  146.3 0.0 collective-permute-start.2
  146.3 0.0 copy-done.5
  146.3 0.0 copy-start.6
  146.3 0.4 convert_reduce_fusion
  146.7 0.7 slice.14
  147.4 0.8 slice.12
  148.3 15.1 %all-to-all-done = bf16[16,128,256]{1,2,0:T(8,128)(2,1)} async-done(((bf16[16,128,256]{1,2,0:T(8,128)(2,1)}), bf16[16,128,256]{1,2,0:T(8,128)(2,1)}, u32[]{:S(2)}, u32[]{:S(2)}) %all-to-all-start) | async-done | bytes 1048608 | tf_op jit(solution)/shard_map/all_to_all | solution.py:428
  163.4 1.4 reduce_sum.42
  164.8 0.1 copy.20
  164.9 1.1 broadcast_in_dim.16
  166.0 4.8 %all-to-all-start.1 = ((bf16[16,128,256]{2,1,0:T(8,128)(2,1)}), bf16[16,128,256]{2,1,0:T(8,128)(2,1)S(1)}, u32[]{:S(2)}, u32[]{:S(2)}) async-start(bf16[16,128,256]{2,1,0:T(8,128)(2,1)} %broadcast_in_dim.16), calls=%async_computation.1 | async-start | bytes 2097152 | tf_op jit(solution)/shard_map/all_to_all | solution.py:435
  170.8 0.0 copy-done.6
  170.8 1.4 fusion.30
  172.2 1.0 fusion.32
  173.3 0.1 collective-permute-start
  173.3 1.5 collective-permute-done
  174.9 0.0 collective-permute-done.1
  174.9 0.0 copy-start.3
  174.9 0.0 copy-start.4
  174.9 0.0 copy-start.7
  174.9 4.0 %fusion.15 = bf16[256,2048]{1,0:T(8,128)(2,1)} fusion(bf16[2048,512]{1,0:T(8,128)(2,1)} %collective-permute-done.1, bf16[2048,256]{1,0:T(8,128)(2,1)S(1)} %copy-done.1, bf16[2048,256]{1,0:T(8,128)(2,1)S(1)} %copy-done.2, bf16[256,512]{1,0:T(8,128)(2,1)S(1)} %collective-permute-done, bf16[256,512]{1,0:T(8,128)(2,1)S(1)} %get-tuple-element.19), kind=kOutput, calls=%fused_computation.15 | convolution fusion | flops 1087897600 | bytes 5767168 | tf_op jit(solution)/shard_map/dot_general | solution.py:421
  178.9 0.0 collective-permute-done.2
  178.9 0.0 collective-permute-done.3
  178.9 0.0 copy-done.3
  178.9 0.0 copy-done.4
  178.9 0.0 copy-done.7
  178.9 8.5 %fusion.12 = bf16[1024,2048]{1,0:T(8,128)(2,1)} fusion(bf16[2048,512]{1,0:T(8,128)(2,1)} %collective-permute-done.3, bf16[2048,256]{1,0:T(8,128)(2,1)S(1)} %copy-done.4, bf16[2048,256]{1,0:T(8,128)(2,1)S(1)} %copy-done.3, bf16[1024,512]{1,0:T(8,128)(2,1)} %collective-permute-done.2, bf16[1024,512]{1,0:T(8,128)(2,1)S(1)} %copy-done.7), kind=kOutput, calls=%fused_computation.13 | convolution fusion | flops 4313841664 | bytes 10485760 | tf_op jit(solution)/shard_map/dot_general | solution.py:421
  187.4 7.6 %all-to-all-done.1 = bf16[16,128,256]{2,1,0:T(8,128)(2,1)S(1)} async-done(((bf16[16,128,256]{2,1,0:T(8,128)(2,1)}), bf16[16,128,256]{2,1,0:T(8,128)(2,1)S(1)}, u32[]{:S(2)}, u32[]{:S(2)}) %all-to-all-start.1) | async-done | bytes 1048608 | tf_op jit(solution)/shard_map/all_to_all | solution.py:435
  195.0 1.5 bitcast_convert_fusion
  (2 shorter events, 0.0 us)
Async XLA Ops:
  131.8 6.6 %copy-start.1 = (bf16[2048,256]{1,0:T(8,128)(2,1)S(1)}, bf16[2048,256]{1,0:T(8,128)(2,1)}, u32[]{:S(2)}) copy-start(bf16[2048,256]{1,0:T(8,128)(2,1)} %wg_hbm.1) | copy-start | bytes 3145732
  131.8 6.6 %copy-start.2 = (bf16[2048,256]{1,0:T(8,128)(2,1)S(1)}, bf16[2048,256]{1,0:T(8,128)(2,1)}, u32[]{:S(2)}) copy-start(bf16[2048,256]{1,0:T(8,128)(2,1)} %wq_hbm.1) | copy-start | bytes 3145732
  133.1 30.4 %all-to-all-start = ((bf16[16,128,256]{1,2,0:T(8,128)(2,1)}), bf16[16,128,256]{1,2,0:T(8,128)(2,1)}, u32[]{:S(2)}, u32[]{:S(2)}) async-start(bf16[16,128,256]{1,2,0:T(8,128)(2,1)} %bitcast.31), calls=%async_computation | async-start | bytes 2097152 | tf_op jit(solution)/shard_map/all_to_all | solution.py:428
  138.4 5.0 %copy-start = (bf16[32,64,256]{2,1,0:T(8,128)(2,1)S(1)}, bf16[32,64,256]{2,1,0:T(8,128)(2,1)}, u32[]{:S(2)}) copy-start(bf16[32,64,256]{2,1,0:T(8,128)(2,1)} %get-tuple-element.16) | copy-start | bytes 3145732
  139.9 35.0 %collective-permute-start.1 = (bf16[2048,512]{1,0:T(8,128)(2,1)}, bf16[2048,512]{1,0:T(8,128)(2,1)}, u32[]{:S(2)}, u32[]{:S(2)}) collective-permute-start(bf16[2048,512]{1,0:T(8,128)(2,1)} %pad_maximum_fusion), channel_id=1, source_target_pairs={{0,1},{1,0},{2,3},{3,2},{4,5},{5,4},{6,7},{7,6},{8,9},{9,8},{10,11... | collective-permute-start | bytes 6291464 | tf_op jit(solution)/shard_map/ppermute | solution.py:351
  142.9 36.0 %collective-permute-start.3 = (bf16[2048,512]{1,0:T(8,128)(2,1)}, bf16[2048,512]{1,0:T(8,128)(2,1)}, u32[]{:S(2)}, u32[]{:S(2)}) collective-permute-start(bf16[2048,512]{1,0:T(8,128)(2,1)} %pad_maximum_fusion.1), channel_id=1, source_target_pairs={{0,1},{1,0},{2,3},{3,2},{4,5},{5,4},{6,7},{7,6},{8,9},{9,8},{10,11... | collective-permute-start | bytes 6291464 | tf_op jit(solution)/shard_map/ppermute | solution.py:351
  143.4 2.9 %copy-start.5 = (bf16[4,2,8,64,256]{4,3,2,1,0:T(8,128)(2,1)S(1)}, bf16[4,2,8,64,256]{4,3,2,1,0:T(8,128)(2,1)}, u32[]{:S(2)}) copy-start(bf16[4,2,8,64,256]{4,3,2,1,0:T(8,128)(2,1)} %get-tuple-element.10) | copy-start | bytes 6291460
  146.3 32.6 %collective-permute-start.2 = (bf16[1024,512]{1,0:T(8,128)(2,1)}, bf16[1024,512]{1,0:T(8,128)(2,1)}, u32[]{:S(2)}, u32[]{:S(2)}) collective-permute-start(bf16[1024,512]{1,0:T(8,128)(2,1)} %get-tuple-element.18), channel_id=1, source_target_pairs={{0,1},{1,0},{2,3},{3,2},{4,5},{5,4},{6,7},{7,6},{8,9},{9,8},{10,11... | collective-permute-start | bytes 3145736 | tf_op jit(solution)/shard_map/ppermute | solution.py:419
  146.3 24.5 %copy-start.6 = (bf16[512,256]{1,0:T(8,128)(2,1)S(1)}, bf16[512,256]{1,0:T(8,128)(2,1)}, u32[]{:S(2)}) copy-start(bf16[512,256]{1,0:T(8,128)(2,1)} %up_hbm.1) | copy-start | bytes 786436
  166.0 29.0 %all-to-all-start.1 = ((bf16[16,128,256]{2,1,0:T(8,128)(2,1)}), bf16[16,128,256]{2,1,0:T(8,128)(2,1)S(1)}, u32[]{:S(2)}, u32[]{:S(2)}) async-start(bf16[16,128,256]{2,1,0:T(8,128)(2,1)} %broadcast_in_dim.16), calls=%async_computation.1 | async-start | bytes 2097152 | tf_op jit(solution)/shard_map/all_to_all | solution.py:435
  173.3 1.6 collective-permute-start
  174.9 4.1 %copy-start.3 = (bf16[2048,256]{1,0:T(8,128)(2,1)S(1)}, bf16[2048,256]{1,0:T(8,128)(2,1)}, u32[]{:S(2)}) copy-start(bf16[2048,256]{1,0:T(8,128)(2,1)} %wk_hbm.1) | copy-start | bytes 3145732
  174.9 4.1 %copy-start.4 = (bf16[2048,256]{1,0:T(8,128)(2,1)S(1)}, bf16[2048,256]{1,0:T(8,128)(2,1)}, u32[]{:S(2)}) copy-start(bf16[2048,256]{1,0:T(8,128)(2,1)} %wv_hbm.1) | copy-start | bytes 3145732
  174.9 4.1 %copy-start.7 = (bf16[1024,512]{1,0:T(8,128)(2,1)S(1)}, bf16[1024,512]{1,0:T(8,128)(2,1)}, u32[]{:S(2)}) copy-start(bf16[1024,512]{1,0:T(8,128)(2,1)} %get-tuple-element.17) | copy-start | bytes 3145732

commit v3 on v2

--- a/solution.py
+++ b/solution.py
@@ -14,17 +14,11 @@
 MESH = pl.DeviceIdType.MESH
 UNROLL = 4
 CHUNKS = 8
+GROUP = 16
 LOW = -1e30
 bf16, f32, i32 = jnp.bfloat16, jnp.float32, jnp.int32
 ANY = pl.BlockSpec(memory_space=pl.ANY)
 VM = pl.BlockSpec(memory_space=pltpu.VMEM)
-
-
-def greet(peers):
-    barrier = pltpu.get_barrier_semaphore()
-    for peer in peers:
-        pl.semaphore_signal(barrier, inc=1, device_id={"st": peer}, device_id_type=MESH)
-    pl.semaphore_wait(barrier, len(peers))
 
 
 def place(depth, plane):
@@ -44,12 +38,13 @@
 
 def core_kernel(
     sizes, mine, hidden_hbm, store_hbm, wq_hbm, wg_hbm, wk_hbm, wv_hbm, up_hbm,
-    tab_out, gate_ref, dk_in, dv_in, part_in,
-    hidden, store, wq, wg, wk, wv, up, q_all, da_all, keys, values, pack_k, pack_v, k_in, v_in,
+    hidden_out, store_out, weight_out,
+    hidden, store, wq, wg, wk, wv, swq, swg, swk, swv, up, gates, q_all, da_all, keys, values, pack_k, pack_v, k_in, v_in,
     score_at, dprob_at, dk_out, dv_out, piece, part_out,
-    tops, sums, mids, marks, block_top, block_sum, block_mid, stat_own, stat_all, tab_v, tab,
-    load_sem, chunk_sem, own_sem, tab_sem, tsend, trecv, qsend, qrecv, asend, arecv, ksend, krecv, vsend, vrecv,
-    ssend, srecv, gksend, gkrecv, gvsend, gvrecv, psend, precv,
+    dk_land, dv_land, part_land, pick, key_sib, value_sib, token, token_sib,
+    grad_w, w_out, w_land, w_plane, z_land, w_all, tops, sums, mids, marks, block_top, block_sum, block_mid, stat_own, stat_all, tab_v, tab,
+    load_sem, chunk_sem, own_sem, tab_sem, wsend, wrecv, sibsend, sibrecv, tsend, trecv, qsend, qrecv, asend, arecv, ksend, krecv, vsend, vrecv,
+    ssend, srecv, gksend, gkrecv, gvsend, gvrecv, psend, precv, rsend, rrecv, zsend, zrecv, csend, crecv, lsend, lrecv,
 ):
     depth, plane, cap, held, requests, per_block = sizes
     me, my_z, my_p, column, row = place(depth, plane)
@@ -65,8 +60,7 @@
             ((hidden_hbm, hidden), (wq_hbm, wq), (wg_hbm, wg), (up_hbm, up), (wk_hbm, wk), (wv_hbm, wv))
         )
     ]
-    for c in loads[:5]:
-        c.start()
+    loads[4].start()
 
     def chunk(c):
         at = pl.ds(pl.multiple_of(c * rows, rows), rows)
@@ -74,8 +68,11 @@
 
     for c in range(CHUNKS):
         chunk(c).start()
-    loads[5].start()
+    for c in loads[:4] + loads[5:]:
+        c.start()
     tab_v[me] = mine[...]
+    half_at = lax.axis_index("tp")
+    other = lax.axis_size("tp") - 1 - half_at
 
     barrier = pltpu.get_barrier_semaphore()
 
@@ -83,7 +80,14 @@
     def _(d):
         pl.semaphore_signal(barrier, inc=1, device_id={"st": (me + d) % owners}, device_id_type=MESH)
 
-    pl.semaphore_wait(barrier, owners - 1)
+    pl.semaphore_signal(barrier, inc=1, device_id={"tp": other}, device_id_type=MESH)
+    pl.semaphore_wait(barrier, owners)
+
+    def sibling(src, dst, send, recv):
+        return pltpu.make_async_remote_copy(
+            src_ref=src, dst_ref=dst, send_sem=send, recv_sem=recv,
+            device_id={"tp": other}, device_id_type=MESH,
+        )
 
     def table_copy(d):
         return remote(mine, tab_v.at[me], tsend.at[d - 1], trecv.at[d - 1], (me + d) % owners)
@@ -91,22 +95,6 @@
     @pl.loop(1, owners)
     def _(d):
         table_copy(d).start()
-
-    loads[0].wait()
-    loads[1].wait()
-    tiles = q_all.shape[1:]
-    q_all[my_z] = jnp.dot(hidden[...], wq[...], preferred_element_type=f32).astype(bf16).reshape(tiles)
-    q_copies = [remote(q_all.at[my_z], q_all.at[my_z], qsend.at[i], qrecv.at[i], p) for i, p in enumerate(column)]
-    for c in q_copies:
-        c.start()
-    loads[2].wait()
-    loads[3].wait()
-    gates = jnp.dot(hidden[...], wg[...], preferred_element_type=f32)
-    gate_ref[...] = gates
-    da_all[my_z] = (up[...].astype(f32) * gates * jax.nn.sigmoid(gates)).astype(bf16).reshape(tiles)
-    a_copies = [remote(da_all.at[my_z], da_all.at[my_z], asend.at[i], arecv.at[i], p) for i, p in enumerate(column)]
-    for c in a_copies:
-        c.start()
 
     def project(weight, out, fetch):
         @pl.loop(0, CHUNKS)
@@ -146,14 +134,51 @@
         table_copy(d).wait()
 
     to_smem = pltpu.make_async_copy(tab_v, tab, tab_sem.at[0])
-    to_out = pltpu.make_async_copy(tab_v, tab_out, tab_sem.at[1])
     to_smem.start()
-    to_out.start()
     to_smem.wait()
     k_copies = spread(keys, pack_k, k_in, ksend, krecv)
+
+    loads[0].wait()
+    loads[1].wait()
+    tiles = q_all.shape[1:]
+    q_all[my_z] = jnp.dot(hidden[...], wq[...], preferred_element_type=f32).astype(bf16).reshape(tiles)
+    q_copies = [remote(q_all.at[my_z], q_all.at[my_z], qsend.at[i], qrecv.at[i], p) for i, p in enumerate(column)]
+    for c in q_copies:
+        c.start()
+    loads[2].wait()
+    loads[3].wait()
+    gates[...] = jnp.dot(hidden[...], wg[...], preferred_element_type=f32)
+    da_all[my_z] = (
+        up[...].astype(f32) * gates[...] * jax.nn.sigmoid(gates[...])
+    ).astype(bf16).reshape(tiles)
+    a_copies = [remote(da_all.at[my_z], da_all.at[my_z], asend.at[i], arecv.at[i], p) for i, p in enumerate(column)]
+    for c in a_copies:
+        c.start()
     loads[5].wait()
     project(wv, values, False)
     v_copies = spread(values, pack_v, v_in, vsend, vrecv)
+    w_copies = [
+        sibling(a, b, wsend.at[i], wrecv.at[i])
+        for i, (a, b) in enumerate(((wq, swq), (wg, swg), (wk, swk), (wv, swv)))
+    ]
+    for c in w_copies:
+        c.start()
+
+    lane = lax.broadcasted_iota(i32, (1, pick.shape[1]), 1)
+
+    def target(n, found):
+        p, zc = n // slots, n % slots
+        code = tab[(zc // cap) * plane + p, 0, me * cap + zc % cap]
+        return jnp.where(lane // GROUP == n, jnp.where(code > 0, (code - 1) % held, -1), found)
+
+    aim = lax.fori_loop(0, plane * slots, target, jnp.full(lane.shape, -1, i32))
+    wanted = aim * GROUP + lane % GROUP
+
+    @pl.loop(0, held)
+    def _(p):
+        line = lax.broadcasted_iota(i32, (GROUP, 1), 0) + p * GROUP
+        at = pl.ds(pl.multiple_of(p * GROUP, GROUP), GROUP)
+        pick[at] = jnp.where((wanted == line) & (aim >= 0), 1.0, 0.0).astype(bf16)
 
     def code_of(z, p, c):
         return tab[z * plane + my_p, 0, (my_z * plane + p) * cap + c]
@@ -233,7 +258,7 @@
     block_sum[...] = inverse
     block_mid[...] = mid * inverse
 
-    back = []
+    p_copies, gv_copies = [], []
     for d in range(1, depth + 1):
         z = (my_z + d) % depth
 
@@ -265,45 +290,158 @@
             for i in range(2):
                 part_out[z, i, b] = sum(piece[f, i] for f in found).astype(bf16)
 
+        if d < depth:
+            p_copies.append(remote(part_out.at[z], part_land.at[my_z], psend.at[d - 1], precv.at[d - 1], column[d - 1]))
+            p_copies[-1].start()
         at = pl.ds(z * cap, cap)
-        if d < depth:
-            back.append(remote(part_out.at[z], part_in.at[my_z], psend.at[d - 1], precv.at[d - 1], column[d - 1]))
-        else:
-            back.append(pltpu.make_async_copy(part_out.at[z], part_in.at[my_z], own_sem.at[0]))
-        back[-1].start()
         for i, peer in enumerate(row):
-            p = peer % plane
             n = (d - 1) * (plane - 1) + i
-            for out, into, send, recv in ((dv_out, dv_in, gvsend, gvrecv), (dk_out, dk_in, gksend, gkrecv)):
-                back.append(remote(out.at[p, at], into.at[my_p, at], send.at[n], recv.at[n], peer))
-                back[-1].start()
-    for i, (out, into) in enumerate(((dv_out, dv_in), (dk_out, dk_in))):
-        back.append(pltpu.make_async_copy(out.at[my_p], into.at[my_p], own_sem.at[1 + i]))
-        back[-1].start()
-    to_out.wait()
-    for c in back:
-        c.wait()
-
-
-def totals_kernel(sizes, table, dk_ref, dv_ref, key_ref, value_ref, acc):
-    depth, plane, cap, held, _, _ = sizes
-    slots = depth * cap
-    me = lax.axis_index("st")
-    acc[...] = jnp.zeros_like(acc)
-
-    @pl.loop(0, plane * slots)
-    def _(s):
-        p, zc = s // slots, s % slots
-        code = table[(zc // cap) * plane + p, 0, me * cap + zc % cap]
-
-        @pl.when(code > 0)
-        def _():
-            at = (code - 1) % held
-            acc[0, at] += dk_ref[p, zc].astype(f32)
-            acc[1, at] += dv_ref[p, zc].astype(f32)
-
-    key_ref[...] = acc[0].astype(bf16)
-    value_ref[...] = acc[1].astype(bf16)
+            gv_copies.append(
+                remote(dv_out.at[peer % plane, at], dv_land.at[my_p, at], gvsend.at[n], gvrecv.at[n], peer)
+            )
+            gv_copies[-1].start()
+
+    def send_keys(n):
+        at = pl.ds(n * (slots // 2), slots // 2)
+        out = []
+        for i, peer in enumerate(row):
+            m = n * (plane - 1) + i
+            out.append(remote(dk_out.at[peer % plane, at], dk_land.at[my_p, at], gksend.at[m], gkrecv.at[m], peer))
+            out[-1].start()
+        return out
+
+    key_low, value_low = keys, values
+    gk_copies = send_keys(0)
+    dk_land[my_p] = dk_out[my_p]
+    dv_land[my_p] = dv_out[my_p]
+    part_land[my_z] = part_out[my_z]
+
+    def totals(land, low):
+        for g in range(span // GROUP):
+            at = slice(g * GROUP, (g + 1) * GROUP)
+            slab = land[:, :, at, :].reshape(plane * slots * GROUP, width)
+            low[:, at, :] = jnp.dot(pick[...], slab, preferred_element_type=f32).astype(bf16).reshape(
+                held, GROUP, width
+            )
+
+    half = held // lax.axis_size("tp")
+
+    def swap(low, sib, n):
+        c = sibling(low.at[pl.ds(other * half, half)], sib, sibsend.at[n], sibrecv.at[n])
+        c.start()
+        return c
+
+    for c in gv_copies:
+        c.wait()
+    totals(dv_land, value_low)
+    swaps = [swap(value_low, value_sib, 0)]
+    model_width = store.shape[1]
+    step = model_width // 4
+
+    @pl.loop(0, 4)
+    def _(n):
+        at = pl.ds(pl.multiple_of(n * step, step), step)
+        grad_w[:, at] = lax.dot_general(
+            value_low[...].reshape(held * span, width), store[:, at], TN, preferred_element_type=f32
+        )
+
+    strip = width // owners
+    for z in range(depth):
+        for p in range(plane):
+            lo = (z * plane + p) * strip
+            w_out[p, z] = grad_w[lo : lo + strip].astype(bf16)
+    r_copies = [
+        remote(w_out.at[peer % plane], w_land.at[i], rsend.at[i], rrecv.at[i], peer) for i, peer in enumerate(row)
+    ]
+    for c in r_copies:
+        c.start()
+    gk_copies += send_keys(1)
+
+    for c in r_copies:
+        c.wait()
+    plane_sum = w_out[my_p].astype(f32)
+    for i in range(plane - 1):
+        plane_sum += w_land[i].astype(f32)
+    w_plane[...] = plane_sum.astype(bf16)
+    z_copies = [
+        remote(w_plane.at[peer // plane], z_land.at[i], zsend.at[i], zrecv.at[i], peer)
+        for i, peer in enumerate(column)
+    ]
+    for c in z_copies:
+        c.start()
+
+    for c in p_copies + w_copies:
+        c.wait()
+    summed = [
+        sum(part_land[z, i].astype(f32) for z in range(depth)).reshape(gates.shape) for i in range(2)
+    ]
+    token[0] = summed[1].astype(bf16).reshape(token.shape[1:])
+    s = jax.nn.sigmoid(gates[...])
+    token[1] = (up[...].astype(f32) * summed[0] * s * (1.0 + gates[...] * (1.0 - s))).astype(bf16).reshape(
+        token.shape[1:]
+    )
+    swap_token = sibling(token.at[:, other], token_sib, sibsend.at[2], sibrecv.at[2])
+    swap_token.start()
+
+    for c in z_copies:
+        c.wait()
+    whole = w_plane[my_z].astype(f32)
+    for i in range(depth - 1):
+        whole += z_land[i].astype(f32)
+    w_all[my_z] = whole.astype(bf16)
+    c_copies = [remote(w_all.at[my_z], w_all.at[my_z], csend.at[i], crecv.at[i], p) for i, p in enumerate(column)]
+    for c in c_copies:
+        c.start()
+
+    def over_heads(mine_rows, sib_rows, own_weights, sib_weights):
+        terms = [
+            lax.dot_general(r, w[...], NT, preferred_element_type=f32)
+            for r, w in zip(mine_rows + sib_rows, own_weights + sib_weights)
+        ]
+        return sum(terms).astype(bf16)
+
+    swap_token.wait()
+    hid = hidden.at[pl.ds(0, hidden_out.shape[0])]
+    hid[...] = over_heads(
+        [token[0, half_at], token[1, half_at]], [token_sib[0], token_sib[1]], [wq, wg], [swq, swg]
+    )
+    outs = [pltpu.make_async_copy(hid, hidden_out, own_sem.at[0])]
+    outs[-1].start()
+
+    for c in c_copies:
+        c.wait()
+    l_copies = [
+        remote(w_all, weight_out.at[:, my_p], lsend.at[i], lrecv.at[i], peer) for i, peer in enumerate(row)
+    ]
+    for c in l_copies:
+        c.start()
+    outs.append(pltpu.make_async_copy(w_all, weight_out.at[:, my_p], own_sem.at[1]))
+    outs[-1].start()
+
+    for c in gk_copies:
+        c.wait()
+    totals(dk_land, key_low)
+    swaps.append(swap(key_low, key_sib, 1))
+    for c in swaps:
+        c.wait()
+    few = half // 4
+    stage = few * span
+
+    @pl.loop(0, 4)
+    def _(n):
+        at = pl.ds(half_at * half + n * few, few)
+        there = pl.ds(n * few, few)
+        pick_rows = lambda ref, where: ref[where].reshape(stage, width)
+        store[pl.ds(pl.multiple_of(n * stage, stage), stage)] = over_heads(
+            [pick_rows(key_low, at), pick_rows(value_low, at)],
+            [pick_rows(key_sib, there), pick_rows(value_sib, there)],
+            [wk, wv], [swk, swv],
+        )
+
+    outs.append(pltpu.make_async_copy(store.at[pl.ds(0, half * span)], store_out, own_sem.at[2]))
+    outs[-1].start()
+    for c in outs + l_copies:
+        c.wait()
 
 
 def body(
@@ -318,7 +456,6 @@
 ):
     owner_count = lax.axis_size("st")
     tp_count = lax.axis_size("tp")
-    tp_index = lax.axis_index("tp")
     depth = 2 ** ((int(math.log2(owner_count)) + 1) // 2)
     plane = owner_count // depth
     held, span, model_width = passage_store.shape
@@ -331,7 +468,6 @@
     slots, mixed = depth * cap, plane * cap
     blocks = depth * block_count
     sizes = (depth, plane, cap, held, requests, per_block)
-    exchange = [(i, tp_count - 1 - i) for i in range(tp_count)]
     sds = jax.ShapeDtypeStruct
 
     ids = passage_ids.reshape(requests)
@@ -346,13 +482,6 @@
     words = -(-entries // lanes) * lanes
     mine_table = jnp.pad(jnp.concatenate([slot_codes, owner_of * cap + rank]), (0, 8 * words - entries)).reshape(8, words)
 
-    def swapped(first, second):
-        both = jnp.concatenate([first, second], axis=1)
-        return jnp.concatenate([both, lax.ppermute(both, "tp", exchange)], axis=1)
-
-    token_weight = swapped(query_weight, gate_weight)
-    row_weight = swapped(key_weight, value_weight)
-
     dma, vm, smem = pltpu.SemaphoreType.DMA, pltpu.VMEM, pltpu.SMEM
     rows = held * span
     slot_block = vm((plane, slots, span, width), bf16)
@@ -360,36 +489,48 @@
     far = dma((depth - 1,))
     each = dma((depth * (plane - 1),))
     stat = vm((depth * mixed, block_rows), f32)
-    table, gates, dk_in, dv_in, part_in = pl.pallas_call(
+    half = held // tp_count
+    strip = width // owner_count
+    each_low = vm((held, span, width), bf16)
+    half_low = vm((half, span, width), bf16)
+    tokens_by = (depth, 2, block_count, block_rows, width)
+    grad_hidden, grad_store, grad_weight = pl.pallas_call(
         functools.partial(core_kernel, sizes),
         in_specs=[VM] + [ANY] * 7,
-        out_specs=[ANY, VM, ANY, ANY, ANY],
+        out_specs=[ANY] * 3,
         out_shape=[
-            sds((owner_count,) + mine_table.shape, i32),
-            sds((tokens, width), f32),
-            sds((plane, slots, span, width), bf16),
-            sds((plane, slots, span, width), bf16),
-            sds((depth, 2, block_count, block_rows, width), bf16),
+            sds((tokens // tp_count, model_width), bf16),
+            sds((half * span, model_width), bf16),
+            sds((depth, plane, strip, model_width), bf16),
         ],
         scratch_shapes=[
             vm((tokens, model_width), bf16), vm((rows, model_width), bf16),
-            *[vm((model_width, width), bf16)] * 4,
-            vm((tokens, width), bf16),
+            *[vm((model_width, width), bf16)] * 8,
+            vm((tokens, width), bf16), vm((tokens, width), f32),
             *[vm((depth, block_count, block_rows, width), bf16)] * 2,
-            *[vm((held, span, width), bf16)] * 2,
+            each_low, each_low,
             *[vm((plane - 1, slots, span, width), bf16)] * 2,
             slot_block, slot_block,
             *[vm((plane, slots, span, block_rows), f32)] * 2,
             slot_block, slot_block,
             vm((mixed + 1, 2, block_rows, width), f32),
-            vm((depth, 2, block_count, block_rows, width), bf16),
+            vm(tokens_by, bf16),
+            slot_block, slot_block, vm(tokens_by, bf16),
+            vm((held * GROUP, plane * slots * GROUP), bf16),
+            half_low, half_low,
+            vm((2, tp_count, tokens // tp_count, width), bf16), vm((2, tokens // tp_count, width), bf16),
+            vm((width, model_width), f32), vm((plane, depth, strip, model_width), bf16),
+            vm((plane - 1, depth, strip, model_width), bf16), vm((depth, strip, model_width), bf16),
+            vm((depth - 1, strip, model_width), bf16), vm((depth, strip, model_width), bf16),
             stat, stat, stat, vm((depth * mixed, block_rows), i32),
             *[vm((blocks, block_rows), f32)] * 3,
             vm((2 * blocks, 2 * block_rows), f32), vm((depth, 2 * blocks, 2 * block_rows), f32),
             vm((owner_count,) + mine_table.shape, i32), smem((owner_count,) + mine_table.shape, i32),
-            dma((6,)), dma((CHUNKS,)), dma((3,)), dma((2,)),
+            dma((6,)), dma((CHUNKS,)), dma((3,)), dma((2,)), dma((4,)), dma((4,)), dma((3,)), dma((3,)),
             dma((owner_count - 1,)), dma((owner_count - 1,)),
-            far, far, far, far, near, near, near, near, far, far, each, each, each, each, far, far,
+            far, far, far, far, near, near, near, near, far, far,
+            dma((2 * (plane - 1),)), dma((2 * (plane - 1),)), each, each, far, far,
+            near, near, far, far, far, far, near, near,
         ],
         compiler_params=pltpu.CompilerParams(collective_id=0, has_side_effects=True, vmem_limit_bytes=63 << 20),
         name="core",
@@ -397,50 +538,11 @@
         mine_table, hidden, passage_store.reshape(rows, model_width),
         query_weight, gate_weight, key_weight, value_weight, output_grad,
     )
-    key_low, value_low = pl.pallas_call(
-        functools.partial(totals_kernel, sizes),
-        in_specs=[pl.BlockSpec(memory_space=smem), VM, VM],
-        out_specs=[VM] * 2,
-        scratch_shapes=[vm((2, held, span, width), f32)],
-        out_shape=[sds((held, span, width), bf16)] * 2,
-        name="totals",
-    )(table, dk_in, dv_in)
-
-    summed = jnp.sum(part_in.astype(f32), axis=0).reshape(2, tokens, width)
-    d_queries = summed[1].astype(bf16)
-    s = jax.nn.sigmoid(gates)
-    d_gates = (output_grad.astype(f32) * summed[0] * s * (1.0 + gates * (1.0 - s))).astype(bf16)
-
-    def over_heads(first, second, weight):
-        both = jnp.concatenate([first, second], axis=1)
-        half = both.shape[0] // tp_count
-        theirs = lax.dynamic_slice_in_dim(both, (tp_count - 1 - tp_index) * half, half, 0)
-        mine = lax.dynamic_slice_in_dim(both, tp_index * half, half, 0)
-        got = lax.ppermute(theirs, "tp", exchange)
-        both = jnp.concatenate([mine, got], axis=1)
-        return lax.dot_general(both, weight, NT, preferred_element_type=f32).astype(bf16)
-
-    grad_hidden = over_heads(d_queries, d_gates, token_weight)
-
-    store_rows = passage_store.reshape(rows, model_width)
-    value_rows = value_low.reshape(rows, width)
-    weight_part = lax.dot_general(store_rows, value_rows, TN, preferred_element_type=f32)
-    parts = lax.all_to_all(
-        weight_part.astype(bf16).reshape(owner_count, model_width // owner_count, width),
-        "st", split_axis=0, concat_axis=0, tiled=True,
-    )
-    weight_sum = jnp.sum(parts.astype(f32), axis=0)
-    shared = jnp.broadcast_to(weight_sum.astype(bf16)[None], parts.shape)
-    grad_value_weight = (
-        lax.all_to_all(shared, "st", split_axis=0, concat_axis=0, tiled=True)
-        .reshape(model_width, width)
-        .astype(f32)
-    )
-
-    grad_store = over_heads(key_low.reshape(rows, width), value_rows, row_weight).reshape(
-        held // tp_count, span, model_width
-    )
-    return (grad_hidden, grad_store, grad_value_weight)
+    return (
+        grad_hidden,
+        grad_store.reshape(half, span, model_width),
+        grad_weight.reshape(width, model_width).T.astype(f32),
+    )
 
 
 def solution(mesh):

time: 197 us -> 155 us (0.79)
  waiting for transfers between devices: 24.3 us -> 0 us
  matrix products: 18.6 us -> 0 us
  Pallas kernels: 123 us -> 141 us
  other arithmetic: 13.5 us -> 1.83 us
  starting transfers between devices: 10.7 us -> 0 us
  local copies, waits for them, and re-layouts: 5.49 us -> 9.02 us
    pallas_call x1, Pallas kernels: 117 us -> 141 us  [body(): pl.pallas_call(functools.partial(core_kernel, sizes), in_specs=[VM] + [AN...]
    all_to_all x2 -> x0, waiting for transfers between devices: 22.8 us -> none  [the longest x1 15.1 us: body(): lax.all_to_all(weight_part.astype(bf16).reshape(owner_count, model_width...]
    dot_general x3 -> x0, matrix products: 18.6 us -> none  [the longest x2 12.5 us: over_heads(): lax.dot_general(both, weight, NT, preferred_element_type=f32).astype(bf16)]
    all_to_all x2 -> x0, starting transfers between devices: 10.1 us -> none  [the longest x1 5.28 us: body(): lax.all_to_all(weight_part.astype(bf16).reshape(owner_count, model_width...]
    concatenate x4 -> x0, other arithmetic: 8.41 us -> none  [the longest x2 4.49 us: swapped(): both = jnp.concatenate([first, second], axis=1)]
    pallas_call x1 -> x0, Pallas kernels: 6.17 us -> none  [body(): pl.pallas_call(functools.partial(totals_kernel, sizes), in_specs=[pl.Bloc...]
    unnamed x17 -> x5, local copies, waits for them, and re-layouts: 0.79 us -> 6.52 us
  transfers between devices with their start and end apart: 6 -> 0, of which waited for: 3 -> 0; matrix products, arithmetic and copies ran while one was open for 14% -> 0% of each run, Pallas kernels for 0% -> 0%
where the time goes in v3:
time: 155 us; the launch traced here: 153 us
  Pallas kernels  141 us (91%)
  local copies, waits for them, and re-layouts  9.02 us (6%)
  other arithmetic  1.83 us (1%)
    pallas_call x1, Pallas kernels, body(): pl.pallas_call(functools.partial(core_kernel, sizes), in_specs=[VM] + [AN...  141 us
    unnamed x5, local copies, waits for them, and re-layouts  6.52 us

profile of v3, /device:TPU:8, one launch (start us, length us, event | category | flops | bytes accessed | tf_op | source)
XLA Modules:
  0.0 152.9 jit_solution(6689057674345279852)
XLA Ops:
  0.6 0.8 copy.15
  1.4 0.1 reshape.117
  1.5 0.2 convert_reduce_fusion
  1.7 0.1 select_reduce_fusion
  1.8 0.1 pad_add_fusion
  1.8 0.6 pad_bitcast_fusion.mine
  2.5 141.4 %core.1 = (bf16[256,2048]{1,0:T(8,128)(2,1)}, bf16[1024,2048]{1,0:T(8,128)(2,1)}, bf16[4,4,16,2048]{3,2,1,0:T(8,128)(2,1)}) custom-call(s32[8,128]{1,0:T(8,128)} %pad_bitcast_fusion.mine, bf16[512,2048]{1,0:T(8,128)(2,1)} %hidden_hbm.1, bf16[2048,2048]{1,0:T(8,128)(2,1)} %bitcast.8, bf16[2048,256]{1,0:T(8,128)(2,1)} %wq_hbm.1, bf16[2048,256]{1,0:T(8,128)(2,1)} %wg_hbm.1, ...), custom_call_target="tpu_custom_call" | custom-call | tf_op jit(solution)/shard_map/core/pallas_call | solution.py:497
  143.8 1.5 bitcast_convert_fusion
  145.3 0.0 copy-start
  145.3 1.8 %copy.16 = f32[256,2048]{0,1:T(8,128)} copy(f32[256,2048]{1,0:T(8,128)S(1)} %bitcast_convert_fusion) | data formatting | bytes 4194304 | tf_op jit(solution)/shard_map/convert_element_type | solution.py:544
  147.1 0.0 copy-done
  147.1 1.0 copy.19
  148.1 4.8 %copy.20 = bf16[16,64,2048]{2,1,0:T(8,128)(2,1)} copy(bf16[16,64,2048]{2,1,0:T(8,128)(2,1)} %bitcast.9) | data formatting | bytes 8388608
  (2 shorter events, 0.0 us)
Async XLA Ops:
  145.3 1.8 %copy-start = (bf16[256,2048]{1,0:T(8,128)(2,1)S(1)}, bf16[256,2048]{1,0:T(8,128)(2,1)}, u32[]{:S(2)}) copy-start(bf16[256,2048]{1,0:T(8,128)(2,1)} %get-tuple-element.14) | copy-start | bytes 3145732

commit v4 on v3

v4 whole, which is shorter than its diff:
```python
import functools
import math

import jax
import jax.numpy as jnp
from jax import lax
from jax.experimental import pallas as pl
from jax.experimental.pallas import tpu as pltpu
from jax.sharding import PartitionSpec as P

HEAD_DIM = 256
NT = (((1,), (1,)), ((), ()))
TN = (((0,), (0,)), ((), ()))
MESH = pl.DeviceIdType.MESH
UNROLL = 4
CHUNKS = 8
FEW = 4
GROUP = 16
WAVES = 2
WIDE = 4
LOW = -1e30
bf16, f32, i32 = jnp.bfloat16, jnp.float32, jnp.int32
ANY = pl.BlockSpec(memory_space=pl.ANY)
VM = pl.BlockSpec(memory_space=pltpu.VMEM)


def div(a, b):
    return lax.div(a, jnp.int32(b))


def rem(a, b):
    return lax.rem(a, jnp.int32(b))


def reader_at(k, depth):
    few = depth // 2
    if isinstance(k, int):
        return 2 * (k % few) + k // few
    return 2 * rem(k, few) + div(k, few)


def place(depth, plane):
    me = lax.axis_index("st")
    my_z, my_p = me // plane, me % plane
    column = [((my_z + d) % depth) * plane + my_p for d in range(1, depth)]
    row = [my_z * plane + (my_p + d) % plane for d in range(1, plane)]
    return me, my_z, my_p, column, row


def remote(src, dst, send, recv, peer):
    return pltpu.make_async_remote_copy(
        src_ref=src, dst_ref=dst, send_sem=send, recv_sem=recv,
        device_id={"st": peer}, device_id_type=MESH,
    )


def core_kernel(
    sizes, ids_hbm, hidden_hbm, store_hbm, wq_hbm, wg_hbm, wk_hbm, wv_hbm, up_hbm,
    hidden_out, store_out, weight_out,
    hidden, store, wq, wg, wk, wv, swq, swg, swk, swv, up, gates, q_all, da_all, keys, values, pack_k, pack_v, k_in, v_in,
    score_at, dprob_at, dk_out, dv_out, piece, part_out,
    dk_land, dv_land, part_land, pick, key_sib, value_sib, token, token_sib,
    grad_w, w_out, w_land, w_plane, z_land, w_all, tops, sums, mids, marks, block_top, block_sum, block_mid, stat_own, stat_all, ids, mine, tab_v, tab,
    load_sem, chunk_sem, own_sem, tab_sem, wsend, wrecv, sibsend, sibrecv, tsend, trecv, qsend, qrecv, asend, arecv, ksend, krecv, vsend, vrecv,
    ssend, srecv, gksend, gkrecv, gvsend, gvrecv, psend, precv, rsend, rrecv, zsend, zrecv, csend, crecv, lsend, lrecv,
):
    depth, plane, cap, held, requests, per_block = sizes
    me, my_z, my_p, column, row = place(depth, plane)
    owners, slots, mixed = depth * plane, depth * cap, plane * cap
    per_reader = requests // per_block
    rows = store.shape[0] // CHUNKS
    span, width = keys.shape[1:]
    passages = rows // span
    scale = HEAD_DIM ** (-0.5)
    ids_copy = pltpu.make_async_copy(ids_hbm, ids, tab_sem.at[1])
    ids_copy.start()
    loads = [
        pltpu.make_async_copy(a, b, load_sem.at[i])
        for i, (a, b) in enumerate(
            ((hidden_hbm, hidden), (wq_hbm, wq), (wg_hbm, wg), (up_hbm, up), (wk_hbm, wk), (wv_hbm, wv))
        )
    ]
    for c in loads[:5]:
        c.start()

    def chunk(c):
        at = pl.ds(pl.multiple_of(c * rows, rows), rows)
        return pltpu.make_async_copy(store_hbm.at[at], store.at[at], chunk_sem.at[c])

    for c in range(CHUNKS):
        chunk(c).start()
    loads[5].start()
    half_at = lax.axis_index("tp")
    other = lax.axis_size("tp") - 1 - half_at

    barrier = pltpu.get_barrier_semaphore()

    @pl.loop(1, owners)
    def _(d):
        pl.semaphore_signal(barrier, inc=1, device_id={"st": (me + d) % owners}, device_id_type=MESH)

    pl.semaphore_signal(barrier, inc=1, device_id={"tp": other}, device_id_type=MESH)

    lane = lax.broadcasted_iota(i32, (requests, tab.shape[2]), 1)
    line = lax.broadcasted_iota(i32, lane.shape, 0)
    wanted, rank = jnp.zeros(lane.shape, i32), jnp.zeros(lane.shape, i32)
    ids_copy.wait()
    each_id = [ids[i // per_block, i % per_block] for i in range(requests)]
    for i, one in enumerate(each_id):
        wanted = jnp.where(line == i, one, wanted)
    owner = div(wanted, held)
    for i, one in enumerate(each_id):
        rank += jnp.where((line > i) & (owner == div(one, held)), 1, 0)
    flat = owner * cap + rank
    code = line * held + rem(wanted, held) + 1
    mine[...] = jnp.sum(
        jnp.where(flat == lane, code, 0) + jnp.where(lane - owners * cap == line, flat, 0), axis=0, keepdims=True
    )
    tab_v[me] = mine[...]

    def sibling(src, dst, send, recv):
        return pltpu.make_async_remote_copy(
            src_ref=src, dst_ref=dst, send_sem=send, recv_sem=recv,
            device_id={"tp": other}, device_id_type=MESH,
        )

    def table_copy(d):
        return remote(mine, tab_v.at[me], tsend.at[d - 1], trecv.at[d - 1], (me + d) % owners)

    def project(weight, out, fetch):
        @pl.loop(0, CHUNKS)
        def _(c):
            if fetch:
                chunk(c).wait()
            part = store[pl.ds(pl.multiple_of(c * rows, rows), rows)]
            out[pl.ds(c * passages, passages)] = jnp.dot(
                part, weight[...], preferred_element_type=f32
            ).astype(bf16).reshape(passages, span, width)

    run = slots // WAVES
    def spread(source, pack, landed, send, recv, wave):
        copies = []
        at = pl.ds(wave * run, run)
        for i in range(plane):
            own = i == plane - 1
            peer_p = my_p if own else row[i] % plane

            @pl.loop(0, run // WIDE)
            def _(t):
                for u in range(WIDE):
                    s = wave * run + t * WIDE + u
                    code = tab[reader_at(div(s, cap), depth) * plane + peer_p, 0, me * cap + rem(s, cap)]
                    value = source[rem(jnp.maximum(code - 1, 0), held)]
                    if own:
                        landed[my_p, s] = value
                    else:
                        pack[i, s] = value

            if not own:
                n = wave * (plane - 1) + i
                copies.append(remote(pack.at[i, at], landed.at[my_p, at], send.at[n], recv.at[n], row[i]))
                copies[-1].start()
        return copies

    loads[0].wait()
    loads[1].wait()
    tiles = q_all.shape[1:]
    q_all[my_z] = jnp.dot(hidden[...], wq[...], preferred_element_type=f32).astype(bf16).reshape(tiles)
    loads[2].wait()
    loads[3].wait()
    gates[...] = jnp.dot(hidden[...], wg[...], preferred_element_type=f32)
    da_all[my_z] = (
        up[...].astype(f32) * gates[...] * jax.nn.sigmoid(gates[...])
    ).astype(bf16).reshape(tiles)
    pl.semaphore_wait(barrier, owners)

    @pl.loop(1, owners)
    def _(d):
        table_copy(d).start()

    q_copies = [remote(q_all.at[my_z], q_all.at[my_z], qsend.at[i], qrecv.at[i], p) for i, p in enumerate(column)]
    a_copies = [remote(da_all.at[my_z], da_all.at[my_z], asend.at[i], arecv.at[i], p) for i, p in enumerate(column)]
    for c in q_copies + a_copies:
        c.start()
    loads[4].wait()
    project(wk, keys, True)

    @pl.loop(1, owners)
    def _(d):
        table_copy(d).wait()

    to_smem = pltpu.make_async_copy(tab_v, tab, tab_sem.at[0])
    to_smem.start()
    to_smem.wait()
    k_copies = [spread(keys, pack_k, k_in, ksend, krecv, 0)]
    loads[5].wait()
    project(wv, values, False)
    v_copies = [spread(values, pack_v, v_in, vsend, vrecv, 0)]
    for wave in range(1, WAVES):
        k_copies.append(spread(keys, pack_k, k_in, ksend, krecv, wave))
        v_copies.append(spread(values, pack_v, v_in, vsend, vrecv, wave))
    w_copies = [
        sibling(a, b, wsend.at[i], wrecv.at[i])
        for i, (a, b) in enumerate(((wq, swq), (wg, swg), (wk, swk), (wv, swv)))
    ]
    for c in w_copies:
        c.start()

    lane = lax.broadcasted_iota(i32, (1, pick.shape[1]), 1)

    def target(n, found):
        p, zc = div(n, slots), rem(n, slots)
        code = tab[reader_at(div(zc, cap), depth) * plane + p, 0, me * cap + rem(zc, cap)]
        return jnp.where(lane // GROUP == n, jnp.where(code > 0, (code - 1) % held, -1), found)

    aim = lax.fori_loop(0, plane * slots, target, jnp.full(lane.shape, -1, i32))
    wanted = aim * GROUP + lane % GROUP

    @pl.loop(0, held)
    def _(p):
        line = lax.broadcasted_iota(i32, (GROUP, 1), 0) + p * GROUP
        at = pl.ds(pl.multiple_of(p * GROUP, GROUP), GROUP)
        pick[at] = jnp.where((wanted == line) & (aim >= 0), 1.0, 0.0).astype(bf16)

    def code_of(z, p, c):
        return tab[z * plane + my_p, 0, (my_z * plane + p) * cap + c]

    def block_of(code):
        return div(div(jnp.maximum(code - 1, 0), held), per_block)

    def slot_at(zc):
        k, c = div(zc, cap), rem(zc, cap)
        return k, reader_at(k, depth), c

    def scores(wave):
        for i in range(plane):
            src = my_p if i == 0 else (my_p + plane - i) % plane
            if i:
                k_copies[wave][i - 1].wait()

            @pl.loop(0, run // WIDE)
            def _(t):
                for u in range(WIDE):
                    zc = wave * run + t * WIDE + u
                    _, z, c = slot_at(zc)
                    q = q_all[z, block_of(code_of(z, src, c))]
                    score_at[src, zc] = lax.dot_general(k_in[src, zc], q, NT, preferred_element_type=f32) * scale

    blocks = depth * per_reader
    group = blocks // WAVES

    def statistics(wave):
        for i in range(plane):
            src = my_p if i == 0 else (my_p + plane - i) % plane
            if i:
                v_copies[wave][i - 1].wait()

            @pl.loop(0, run // WIDE)
            def _(t):
                for u in range(WIDE):
                    zc = wave * run + t * WIDE + u
                    k, z, c = slot_at(zc)
                    code = code_of(z, src, c)
                    block = block_of(code)
                    d_probs = lax.dot_general(v_in[src, zc], da_all[z, block], NT, preferred_element_type=f32)
                    dprob_at[src, zc] = d_probs
                    found = score_at[src, zc]
                    top = jnp.max(found, axis=0, keepdims=True)
                    e = jnp.exp(found - top)
                    at = pl.ds(k * mixed + src * cap + c, 1)
                    tops[at, :] = top
                    sums[at, :] = jnp.sum(e, axis=0, keepdims=True)
                    mids[at, :] = jnp.sum(e * d_probs, axis=0, keepdims=True)
                    marks[at, :] = jnp.full(top.shape, jnp.where(code > 0, block, -1), i32)

        for k in range(wave * depth // WAVES, (wave + 1) * depth // WAVES):
            at = slice(k * mixed, (k + 1) * mixed)
            m, l, c, mark = tops[at], sums[at], mids[at], marks[at]
            for b in range(per_reader):
                on = mark == b
                top = jnp.max(jnp.where(on, m, LOW), axis=0, keepdims=True)
                ratio = jnp.where(on, jnp.exp(jnp.minimum(m - top, 0.0)), 0.0)
                to = slice(k * per_reader + b, k * per_reader + b + 1)
                block_top[to, :] = top
                block_sum[to, :] = jnp.sum(l * ratio, axis=0, keepdims=True)
                block_mid[to, :] = jnp.sum(c * ratio, axis=0, keepdims=True)
        at = slice(wave * group, (wave + 1) * group)
        stat_own[wave, 0:group] = jnp.concatenate([block_top[at], block_sum[at]], axis=1)
        stat_own[wave, group:] = jnp.concatenate([block_mid[at], block_mid[at]], axis=1)
        copies = []
        for i, peer in enumerate(column):
            n = wave * (depth - 1) + i
            copies.append(remote(stat_own.at[wave], stat_all.at[my_z, wave], ssend.at[n], srecv.at[n], peer))
            copies[-1].start()
        stat_all[my_z, wave] = stat_own[wave]
        return copies

    def merge(wave, copies):
        for c in copies:
            c.wait()
        heads = [stat_all[z, wave, 0:group, 0:span] for z in range(depth)]
        top = functools.reduce(jnp.maximum, heads)
        ratios = [jnp.exp(h - top) for h in heads]
        total = sum(stat_all[z, wave, 0:group, span:] * ratios[z] for z in range(depth))
        mid = sum(stat_all[z, wave, group:, 0:span] * ratios[z] for z in range(depth))
        inverse = 1.0 / total
        at = slice(wave * group, (wave + 1) * group)
        block_top[at] = top
        block_sum[at] = inverse
        block_mid[at] = mid * inverse

    gv_copies = []

    def gradients(k):
        z = reader_at(k, depth)

        @pl.loop(0, mixed // UNROLL)
        def _(t):
            for u in range(UNROLL):
                idx = t * UNROLL + u
                p, c = div(idx, cap), rem(idx, cap)
                zc = k * cap + c
                code = code_of(z, p, c)
                block = block_of(code)
                at = pl.ds(k * per_reader + block, 1)
                top = jnp.where(code > 0, block_top[at, :], -LOW)
                probs = jnp.exp(score_at[p, zc] - top) * block_sum[at, :]
                low = probs.astype(bf16)
                d_scores = (probs * (dprob_at[p, zc] - block_mid[at, :]) * scale).astype(bf16)
                dk_out[p, zc] = jnp.dot(d_scores, q_all[z, block], preferred_element_type=f32).astype(bf16)
                dv_out[p, zc] = jnp.dot(low, da_all[z, block], preferred_element_type=f32).astype(bf16)
                piece[idx, 0] = lax.dot_general(low, v_in[p, zc], TN, preferred_element_type=f32)
                piece[idx, 1] = lax.dot_general(d_scores, k_in[p, zc], TN, preferred_element_type=f32)

        at = pl.ds(k * cap, cap)
        for i, peer in enumerate(row):
            n = k * (plane - 1) + i
            gv_copies.append(
                remote(dv_out.at[peer % plane, at], dv_land.at[my_p, at], gvsend.at[n], gvrecv.at[n], peer)
            )
            gv_copies[-1].start()

        @pl.loop(0, per_reader)
        def _(b):
            found = []
            for j in range(per_block):
                flat = tab[z * plane + my_p, 0, owners * cap + b * per_block + j]
                near = div(flat, mixed) == my_z
                found.append(jnp.where(near, rem(flat, mixed), mixed))
            for i in range(2):
                part_out[z, i, b] = sum(piece[f, i] for f in found).astype(bf16)

    for i in range(2):
        piece[mixed, i] = jnp.zeros(piece.shape[2:], f32)
    for c in q_copies:
        c.wait()
    for wave in range(WAVES):
        scores(wave)
        if wave == 0:
            for c in a_copies:
                c.wait()
        merge(wave, statistics(wave))
        for k in range(wave * depth // WAVES, (wave + 1) * depth // WAVES):
            gradients(k)

    def send_keys(n):
        at = pl.ds(n * run, run)
        out = []
        for i, peer in enumerate(row):
            m = n * (plane - 1) + i
            out.append(remote(dk_out.at[peer % plane, at], dk_land.at[my_p, at], gksend.at[m], gkrecv.at[m], peer))
            out[-1].start()
        return out

    key_low, value_low = keys, values
    p_copies = [
        remote(part_out.at[peer // plane], part_land.at[my_z], psend.at[i], precv.at[i], peer)
        for i, peer in enumerate(column)
    ]
    for c in p_copies[:-1]:
        c.start()
    gk_copies = send_keys(0)
    dk_land[my_p] = dk_out[my_p]
    dv_land[my_p] = dv_out[my_p]
    part_land[my_z] = part_out[my_z]

    def totals(land, low):
        for g in range(span // GROUP):
            at = slice(g * GROUP, (g + 1) * GROUP)
            slab = land[:, :, at, :].reshape(plane * slots * GROUP, width)
            low[:, at, :] = jnp.dot(pick[...], slab, preferred_element_type=f32).astype(bf16).reshape(
                held, GROUP, width
            )

    half = held // lax.axis_size("tp")

    def swap(low, sib, n):
        c = sibling(low.at[pl.ds(other * half, half)], sib, sibsend.at[n], sibrecv.at[n])
        c.start()
        return c

    for c in gv_copies:
        c.wait()
    totals(dv_land, value_low)
    swaps = [swap(value_low, value_sib, 0)]
    model_width = store.shape[1]
    step = model_width // 4

    @pl.loop(0, 4)
    def _(n):
        at = pl.ds(pl.multiple_of(n * step, step), step)
        grad_w[:, at] = lax.dot_general(
            value_low[...].reshape(held * span, width), store[:, at], TN, preferred_element_type=f32
        )

    strip = width // owners
    for z in range(depth):
        for p in range(plane):
            lo = (z * plane + p) * strip
            w_out[p, z] = grad_w[lo : lo + strip].astype(bf16)
    turns = [(my_z + d) % depth for d in range(1, depth + 1)]
    r_copies = []
    for d, z in enumerate(turns):
        for i, peer in enumerate(row):
            n = d * (plane - 1) + i
            r_copies.append(remote(w_out.at[peer % plane, z], w_land.at[i, z], rsend.at[n], rrecv.at[n], peer))
            r_copies[-1].start()
    for n in range(1, WAVES):
        gk_copies += send_keys(n)

    z_copies = []
    for d, z in enumerate(turns):
        for c in r_copies[d * (plane - 1) : (d + 1) * (plane - 1)]:
            c.wait()
        plane_sum = w_out[my_p, z].astype(f32)
        for i in range(plane - 1):
            plane_sum += w_land[i, z].astype(f32)
        if d < depth - 1:
            w_plane[z] = plane_sum.astype(bf16)
            z_copies.append(remote(w_plane.at[z], z_land.at[d], zsend.at[d], zrecv.at[d], column[d]))
            z_copies[-1].start()
    whole = plane_sum
    for c in z_copies:
        c.wait()
    for i in range(depth - 1):
        whole += z_land[i].astype(f32)
    w_all[my_z] = whole.astype(bf16)
    c_copies = [remote(w_all.at[my_z], w_all.at[my_z], csend.at[i], crecv.at[i], p) for i, p in enumerate(column)]
    for c in c_copies:
        c.start()
    l_copies = []

    def hand_on(d, z):
        for i, peer in enumerate(row):
            n = d * (plane - 1) + i
            l_copies.append(remote(w_all.at[z], weight_out.at[z, my_p], lsend.at[n], lrecv.at[n], peer))
            l_copies[-1].start()

    hand_on(0, my_z)
    p_copies[-1].start()
    for d, c in enumerate(c_copies):
        c.wait()
        hand_on(d + 1, (my_z + depth - d - 1) % depth)
    outs = [pltpu.make_async_copy(w_all, weight_out.at[:, my_p], own_sem.at[1])]
    outs[-1].start()

    def over_heads(mine_rows, sib_rows, own_weights, sib_weights):
        terms = [
            lax.dot_general(r, w[...], NT, preferred_element_type=f32)
            for r, w in zip(mine_rows + sib_rows, own_weights + sib_weights)
        ]
        return sum(terms).astype(bf16)

    for c in gk_copies + w_copies:
        c.wait()
    totals(dk_land, key_low)
    swaps.append(swap(key_low, key_sib, 1))
    for c in swaps:
        c.wait()
    few = half // 4
    stage = few * span

    @pl.loop(0, 4)
    def _(n):
        at = pl.ds(half_at * half + n * few, few)
        there = pl.ds(n * few, few)
        pick_rows = lambda ref, where: ref[where].reshape(stage, width)
        store[pl.ds(pl.multiple_of(n * stage, stage), stage)] = over_heads(
            [pick_rows(key_low, at), pick_rows(value_low, at)],
            [pick_rows(key_sib, there), pick_rows(value_sib, there)],
            [wk, wv], [swk, swv],
        )

    outs.append(pltpu.make_async_copy(store.at[pl.ds(0, half * span)], store_out, own_sem.at[2]))
    outs[-1].start()

    for c in p_copies:
        c.wait()
    summed = [
        sum(part_land[z, i].astype(f32) for z in range(depth)).reshape(gates.shape) for i in range(2)
    ]
    token[0] = summed[1].astype(bf16).reshape(token.shape[1:])
    s = jax.nn.sigmoid(gates[...])
    token[1] = (up[...].astype(f32) * summed[0] * s * (1.0 + gates[...] * (1.0 - s))).astype(bf16).reshape(
        token.shape[1:]
    )
    swap_token = sibling(token.at[:, other], token_sib, sibsend.at[2], sibrecv.at[2])
    swap_token.start()
    swap_token.wait()
    hid = hidden.at[pl.ds(0, hidden_out.shape[0])]
    hid[...] = over_heads(
        [token[0, half_at], token[1, half_at]], [token_sib[0], token_sib[1]], [wq, wg], [swq, swg]
    )
    outs.append(pltpu.make_async_copy(hid, hidden_out, own_sem.at[0]))
    outs[-1].start()
    for c in outs + l_copies:
        c.wait()


def finish_kernel(hidden_in, store_in, weight_in, hidden_out, store_out, weight_out, hid, store, weight, wide, in_sem, out_sem):
    rows = store_in.shape[0] // CHUNKS
    cols = weight_in.shape[1] // FEW
    pieces = [
        pltpu.make_async_copy(weight_in, weight, in_sem.at[0]),
        pltpu.make_async_copy(hidden_in, hid, in_sem.at[1]),
    ]
    outs = [pltpu.make_async_copy(hid, hidden_out, out_sem.at[0])]
    for n in range(CHUNKS):
        at = pl.ds(n * rows, rows)
        pieces.append(pltpu.make_async_copy(store_in.at[at], store.at[at], in_sem.at[2 + n]))
        outs.append(pltpu.make_async_copy(store.at[at], store_out.at[at], out_sem.at[1 + n]))
    for c in pieces:
        c.start()
    for c, out in zip(pieces[1:5], outs[:4]):
        c.wait()
        out.start()
    pieces[0].wait()
    for n in range(FEW):
        at = pl.ds(n * cols, cols)
        wide[at] = weight[:, n * cols : (n + 1) * cols].astype(f32).T
        outs.append(pltpu.make_async_copy(wide.at[at], weight_out.at[at], out_sem.at[1 + CHUNKS + n]))
        outs[-1].start()
    for c, out in zip(pieces[5:], outs[4 : 1 + CHUNKS]):
        c.wait()
        out.start()
    for c in outs:
        c.wait()


def body(
    hidden,
    passage_store,
    passage_ids,
    query_weight,
    gate_weight,
    key_weight,
    value_weight,
    output_grad,
):
    owner_count = lax.axis_size("st")
    tp_count = lax.axis_size("tp")
    depth = 2 ** ((int(math.log2(owner_count)) + 1) // 2)
    plane = owner_count // depth
    held, span, model_width = passage_store.shape
    block_count, per_block = passage_ids.shape
    requests = block_count * per_block
    cap = max(1, 2 * requests // owner_count)
    width = query_weight.shape[1]
    tokens = hidden.shape[0]
    block_rows = tokens // block_count
    slots, mixed = depth * cap, plane * cap
    blocks = depth * block_count
    sizes = (depth, plane, cap, held, requests, per_block)
    sds = jax.ShapeDtypeStruct

    lanes = 128
    words = -(-(owner_count * cap + requests) // lanes) * lanes

    dma, vm, smem = pltpu.SemaphoreType.DMA, pltpu.VMEM, pltpu.SMEM
    rows = held * span
    slot_block = vm((plane, slots, span, width), bf16)
    near = dma((plane - 1,))
    far = dma((depth - 1,))
    each = dma((depth * (plane - 1),))
    near2, far2 = dma((WAVES * (plane - 1),)), dma((WAVES * (depth - 1),))
    stat = vm((depth * mixed, block_rows), f32)
    half = held // tp_count
    strip = width // owner_count
    each_low = vm((held, span, width), bf16)
    half_low = vm((half, span, width), bf16)
    tokens_by = (depth, 2, block_count, block_rows, width)
    grad_hidden, grad_store, grad_weight = pl.pallas_call(
        functools.partial(core_kernel, sizes),
        in_specs=[ANY] * 8,
        out_specs=[ANY] * 3,
        out_shape=[
            sds((tokens // tp_count, model_width), bf16),
            sds((half * span, model_width), bf16),
            sds((depth, plane, strip, model_width), bf16),
        ],
        scratch_shapes=[
            vm((tokens, model_width), bf16), vm((rows, model_width), bf16),
            *[vm((model_width, width), bf16)] * 8,
            vm((tokens, width), bf16), vm((tokens, width), f32),
            *[vm((depth, block_count, block_rows, width), bf16)] * 2,
            each_low, each_low,
            *[vm((plane - 1, slots, span, width), bf16)] * 2,
            slot_block, slot_block,
            *[vm((plane, slots, span, block_rows), f32)] * 2,
            slot_block, slot_block,
            vm((mixed + 1, 2, block_rows, width), f32),
            vm(tokens_by, bf16),
            slot_block, slot_block, vm(tokens_by, bf16),
            vm((held * GROUP, plane * slots * GROUP), bf16),
            half_low, half_low,
            vm((2, tp_count, tokens // tp_count, width), bf16), vm((2, tokens // tp_count, width), bf16),
            vm((width, model_width), f32), vm((plane, depth, strip, model_width), bf16),
            vm((plane - 1, depth, strip, model_width), bf16), vm((depth, strip, model_width), bf16),
            vm((depth - 1, strip, model_width), bf16), vm((depth, strip, model_width), bf16),
            stat, stat, stat, vm((depth * mixed, block_rows), i32),
            *[vm((blocks, block_rows), f32)] * 3,
            vm((WAVES, 2 * blocks // WAVES, 2 * block_rows), f32),
            vm((depth, WAVES, 2 * blocks // WAVES, 2 * block_rows), f32),
            smem(passage_ids.shape, i32), vm((1, words), i32),
            vm((owner_count, 1, words), i32), smem((owner_count, 1, words), i32),
            dma((6,)), dma((CHUNKS,)), dma((3,)), dma((2,)), dma((4,)), dma((4,)), dma((3,)), dma((3,)),
            dma((owner_count - 1,)), dma((owner_count - 1,)),
            far, far, far, far, near2, near2, near2, near2, far2, far2, near2, near2, each, each, far, far,
            each, each, far, far, far, far, each, each,
        ],
        compiler_params=pltpu.CompilerParams(collective_id=0, has_side_effects=True, vmem_limit_bytes=63 << 20),
        name="core",
    )(
        passage_ids, hidden, passage_store.reshape(rows, model_width),
        query_weight, gate_weight, key_weight, value_weight, output_grad,
    )
    grad_hidden, grad_store, grad_weight = pl.pallas_call(
        finish_kernel,
        in_specs=[ANY] * 3,
        out_specs=[ANY] * 3,
        out_shape=[
            sds(grad_hidden.shape, bf16), sds(grad_store.shape, bf16), sds((model_width, width), f32)
        ],
        scratch_shapes=[
            vm(grad_hidden.shape, bf16), vm(grad_store.shape, bf16),
            vm((width, model_width), bf16), vm((model_width, width), f32),
            dma((2 + CHUNKS,)), dma((1 + CHUNKS + FEW,)),
        ],
        name="finish",
    )(grad_hidden, grad_store, grad_weight.reshape(width, model_width))
    return grad_hidden, grad_store.reshape(half, span, model_width), grad_weight


def solution(mesh):
    placed = (
        P("st", None),
        P("st", None, None),
        P("st", None),
        P(None, "tp"),
        P(None, "tp"),
        P(None, "tp"),
        P(None, "tp"),
        P("st", "tp"),
    )
    return jax.shard_map(
        body,
        mesh=mesh,
        in_specs=placed,
        out_specs=(P(("st", "tp"), None), P(("st", "tp"), None, None), P(None, "tp")),
        check_vma=False,
    )
```

time: 155 us -> 150 us (0.968)
  local copies, waits for them, and re-layouts: 9.02 us -> 1.35 us
  Pallas kernels: 141 us -> 146 us
  other arithmetic: 1.83 us -> 0 us
    unnamed x5 -> x1, local copies, waits for them, and re-layouts: 6.52 us -> 1.35 us
    pallas_call x1 -> x2, Pallas kernels: 141 us -> 146 us  [the longest x1 142 us: body(): pl.pallas_call(functools.partial(core_kernel, sizes), in_specs=[ANY] * 8,...]
    convert_element_type x1 -> x0, local copies, waits for them, and re-layouts: 1.81 us -> none  [body(): grad_weight.reshape(width, model_width).T.astype(f32)]
where the time goes in v4:
time: 150 us; the launch traced here: 148 us
  Pallas kernels  146 us (97%)
    pallas_call x1, Pallas kernels, body(): pl.pallas_call(functools.partial(core_kernel, sizes), in_specs=[ANY] * 8,...  142 us
    pallas_call x1, Pallas kernels, body(): pl.pallas_call(finish_kernel, in_specs=[ANY] * 3, out_specs=[ANY] * 3, ou...  4.71 us

profile of v4, /device:TPU:8, one launch (start us, length us, event | category | flops | bytes accessed | tf_op | source)
XLA Modules:
  0.0 148.3 jit_solution(14807270216112100271)
XLA Ops:
  0.6 1.3 copy.11.ids_hbm
  2.0 141.6 %core.1 = (bf16[256,2048]{1,0:T(8,128)(2,1)}, bf16[1024,2048]{1,0:T(8,128)(2,1)}, bf16[4,4,16,2048]{3,2,1,0:T(8,128)(2,1)}) custom-call(s32[8,4]{1,0:T(8,128)} %copy.11.ids_hbm, bf16[512,2048]{1,0:T(8,128)(2,1)} %hidden_hbm.1, bf16[2048,2048]{1,0:T(8,128)(2,1)} %bitcast.3, bf16[2048,256]{1,0:T(8,128)(2,1)} %wq_hbm.1, bf16[2048,256]{1,0:T(8,128)(2,1)} %wg_hbm.1, ...), custom_call_target="tpu_custom_call" | custom-call | tf_op jit(solution)/shard_map/core/pallas_call | solution.py:592
  143.6 4.7 %finish.1 = (bf16[256,2048]{1,0:T(8,128)(2,1)}, bf16[1024,2048]{1,0:T(8,128)(2,1)}, f32[2048,256]{1,0:T(8,128)}) custom-call(bf16[256,2048]{1,0:T(8,128)(2,1)} %get-tuple-element.9.hidden_in, bf16[1024,2048]{1,0:T(8,128)(2,1)} %get-tuple-element.10.store_in, bf16[256,2048]{1,0:T(8,128)(2,1)} %bitcast.4), custom_call_target="tpu_custom_call" | custom-call | tf_op jit(solution)/shard_map/finish/pallas_call | solution.py:637

commit v5 on v4

--- a/solution.py
+++ b/solution.py
@@ -12,7 +12,7 @@
 NT = (((1,), (1,)), ((), ()))
 TN = (((0,), (0,)), ((), ()))
 MESH = pl.DeviceIdType.MESH
-UNROLL = 4
+UNROLL = 8
 CHUNKS = 8
 FEW = 4
 GROUP = 16
@@ -162,6 +162,12 @@
                 copies[-1].start()
         return copies
 
+    pl.semaphore_wait(barrier, owners)
+
+    @pl.loop(1, owners)
+    def _(d):
+        table_copy(d).start()
+
     loads[0].wait()
     loads[1].wait()
     tiles = q_all.shape[1:]
@@ -172,12 +178,6 @@
     da_all[my_z] = (
         up[...].astype(f32) * gates[...] * jax.nn.sigmoid(gates[...])
     ).astype(bf16).reshape(tiles)
-    pl.semaphore_wait(barrier, owners)
-
-    @pl.loop(1, owners)
-    def _(d):
-        table_copy(d).start()
-
     q_copies = [remote(q_all.at[my_z], q_all.at[my_z], qsend.at[i], qrecv.at[i], p) for i, p in enumerate(column)]
     a_copies = [remote(da_all.at[my_z], da_all.at[my_z], asend.at[i], arecv.at[i], p) for i, p in enumerate(column)]
     for c in q_copies + a_copies:
@@ -373,12 +373,22 @@
         return out
 
     key_low, value_low = keys, values
-    p_copies = [
-        remote(part_out.at[peer // plane], part_land.at[my_z], psend.at[i], precv.at[i], peer)
-        for i, peer in enumerate(column)
-    ]
-    for c in p_copies[:-1]:
-        c.start()
+    def part_copy(z):
+        d = (z + depth - my_z) % depth
+        return remote(part_out.at[z], part_land.at[my_z], psend.at[d - 1], precv.at[d - 1], z * plane + my_p)
+
+    def send_part(z, on):
+        @pl.when(on & (z >= 0) & (z < depth))
+        def _():
+            part_copy(z).start()
+
+    middle = depth // 2
+    for far in range(depth - 1, 0, -1):
+        later = (my_z + (my_z + far) == 2 * middle - 1) if far == 1 else False
+        send_part(my_z + far, jnp.logical_not(later))
+        later = (my_z + (my_z - far) == 2 * middle - 1) if far == 1 else False
+        send_part(my_z - far, jnp.logical_not(later))
+    p_copies = [part_copy((my_z + d) % depth) for d in range(1, depth)]
     gk_copies = send_keys(0)
     dk_land[my_p] = dk_out[my_p]
     dv_land[my_p] = dv_out[my_p]
@@ -457,7 +467,8 @@
             l_copies[-1].start()
 
     hand_on(0, my_z)
-    p_copies[-1].start()
+    send_part(my_z + 1, my_z == middle - 1)
+    send_part(my_z - 1, my_z == middle)
     for d, c in enumerate(c_copies):
         c.wait()
         hand_on(d + 1, (my_z + depth - d - 1) % depth)

time: 150 us -> 142 us (0.947)
  Pallas kernels: 146 us -> 138 us
    pallas_call x1, Pallas kernels: 142 us -> 133 us  [body(): pl.pallas_call(functools.partial(core_kernel, sizes), in_specs=[ANY] * 8,...]
where the time goes in v5:
time: 142 us; the launch traced here: 140 us
  Pallas kernels  138 us (97%)
    pallas_call x1, Pallas kernels, body(): pl.pallas_call(functools.partial(core_kernel, sizes), in_specs=[ANY] * 8,...  133 us
    pallas_call x1, Pallas kernels, body(): pl.pallas_call(finish_kernel, in_specs=[ANY] * 3, out_specs=[ANY] * 3, ou...  4.71 us

profile of v5, /device:TPU:8, one launch (start us, length us, event | category | flops | bytes accessed | tf_op | source)
XLA Modules:
  0.0 140.0 jit_solution(4476902970600214758)
XLA Ops:
  0.6 1.3 copy.11.ids_hbm
  2.0 133.4 %core.1 = (bf16[256,2048]{1,0:T(8,128)(2,1)}, bf16[1024,2048]{1,0:T(8,128)(2,1)}, bf16[4,4,16,2048]{3,2,1,0:T(8,128)(2,1)}) custom-call(s32[8,4]{1,0:T(8,128)} %copy.11.ids_hbm, bf16[512,2048]{1,0:T(8,128)(2,1)} %hidden_hbm.1, bf16[2048,2048]{1,0:T(8,128)(2,1)} %bitcast.3, bf16[2048,256]{1,0:T(8,128)(2,1)} %wq_hbm.1, bf16[2048,256]{1,0:T(8,128)(2,1)} %wg_hbm.1, ...), custom_call_target="tpu_custom_call" | custom-call | tf_op jit(solution)/shard_map/core/pallas_call | solution.py:603
  135.3 4.7 %finish.1 = (bf16[256,2048]{1,0:T(8,128)(2,1)}, bf16[1024,2048]{1,0:T(8,128)(2,1)}, f32[2048,256]{1,0:T(8,128)}) custom-call(bf16[256,2048]{1,0:T(8,128)(2,1)} %get-tuple-element.9.hidden_in, bf16[1024,2048]{1,0:T(8,128)(2,1)} %get-tuple-element.10.store_in, bf16[256,2048]{1,0:T(8,128)(2,1)} %bitcast.4), custom_call_target="tpu_custom_call" | custom-call | tf_op jit(solution)/shard_map/finish/pallas_call | solution.py:648
